TPU v7x, 32 devices: a whole 2x2x4 slice. The times are simulated.
32 devices in a mesh: tp: 8 (over z, y), dp: 4 (over x, core).
Axes of the slice: x: 2, y: 2, z: 4, core: 2. Of those that a mesh axis runs over, the one named last changes fastest.
Arguments:
- tokens: bfloat16 [32, 16, 4096], P('tp', None, 'dp'), may hold values from -24 to 24
- lengths: int32 [32], P('dp'), may hold values from 1 to 16, 224 in all
- norm_gain: float32 [2, 4096], P(None, 'dp'), may hold values from 0.1 to 1.9
- query_weight: bfloat16 [2, 4096, 4096], P(None, 'dp', 'tp'), may hold values from -0.09375 to 0.09375
- key_weight: bfloat16 [2, 4096, 4096], P(None, 'dp', 'tp'), may hold values from -0.09375 to 0.09375
- value_weight: bfloat16 [2, 4096, 4096], P(None, 'dp', 'tp'), may hold values from -0.09375 to 0.09375
- outgate_weight: bfloat16 [2, 4096, 4096], P(None, 'dp', 'tp'), may hold values from -0.09375 to 0.09375
- input_gate_weight: bfloat16 [2, 4096, 32], replicated, may hold values from -0.09375 to 0.09375
- forget_gate_weight: bfloat16 [2, 4096, 32], replicated, may hold values from -0.09375 to 0.09375
- forget_bias: float32 [2, 32], P(None, 'tp'), may hold values from -1 to 6
- out_weight: bfloat16 [2, 4096, 4096], P(None, 'tp', 'dp'), may hold values from -0.09375 to 0.09375
- cell_state: float32 [2, 32, 32, 128, 128], P(None, 'dp', 'tp'), may hold values from -1.5 to 1.5
- norm_state: float32 [2, 32, 32, 128], P(None, 'dp', 'tp'), may hold values from -1.5 to 1.5
- max_state: float32 [2, 32, 32], P(None, 'dp', 'tp'), may hold values from -6 to 6
Outputs:
- tokens_next: bfloat16 [32, 16, 4096], P('tp', None, 'dp')
- cell_next: float32 [2, 32, 32, 128, 128], P(None, 'dp', 'tp')
- norm_next: float32 [2, 32, 32, 128], P(None, 'dp', 'tp')
- max_next: float32 [2, 32, 32], P(None, 'dp', 'tp')
Inputs may be any that keep to these rules, and one draw needn't show every extreme that they name: `lengths`: the largest is 16.
All inputs are finite; a program needn't handle non-finite values. No bound on the sum of `lengths` on one device may be relied on, other than what follows from the above.
Results may differ from a plain program's by a relative error of at most 0.025.
Values may be sent and summed in bfloat16 or wider, within the bound.
A program may use at most 64 MiB of HBM per device.

v0:
```python
import functools
import jax
import jax.numpy as jnp
from jax import lax
from jax.experimental import pallas as pl
from jax.experimental.pallas import tpu as pltpu
from jax.sharding import PartitionSpec as P

EPSILON = 1e-06
NEG_FILL = -1e30
LANES = 128
HIGH = lax.Precision.HIGHEST
BF16 = jnp.bfloat16
F32 = jnp.float32
MESH = pl.DeviceIdType.MESH


def pack_squares(block):
    lane = lax.broadcasted_iota(jnp.int32, block.shape, 1)
    square = jnp.sum(jnp.where(lane >= LANES - 3, block, 0.0), axis=1, keepdims=True)
    first = square.astype(BF16).astype(F32)
    rest = square - first
    second = rest.astype(BF16).astype(F32)
    third = rest - second
    block = jnp.where(lane == LANES - 3, first, block)
    block = jnp.where(lane == LANES - 2, second, block)
    return jnp.where(lane == LANES - 1, third, block).astype(BF16)


def kernel(
    sizes,
    lengths,
    tokens,
    gain,
    weight_q,
    weight_k,
    weight_v,
    weight_o,
    weight_in,
    weight_forget,
    bias,
    weight_out,
    cell_in,
    norm_in,
    max_in,
    tokens_out,
    cell_out,
    norm_out,
    max_out,
    current,
    wts,
    wgate,
    wout,
    cells,
    pad,
    gathered,
    scaled,
    own_main,
    own_gate,
    send1,
    send1g,
    recv1,
    recv1g,
    send2,
    send2g,
    recv2,
    recv2g,
    heads_buf,
    gated,
    mixed,
    mixed_s,
    mixed_y,
    mixed_in,
    load_sem,
    cell_sem,
    gat_s,
    gat_r,
    gfw_s,
    gfw_r,
    one_s,
    one_r,
    two_s,
    two_r,
    gg_s,
    gg_r,
    fw_s,
    fw_r,
    mix_s,
    mix_r,
    my_s,
    my_r,
):
    n_tp, n_dp, span, heads, size = sizes
    chips = n_dp // 2
    my_tp, my_dp = lax.axis_index("tp"), lax.axis_index("dp")
    my_x, my_core = my_dp // 2, lax.rem(my_dp, 2)
    peer_core = 1 - my_core
    peer = my_x * 2 + peer_core
    own_rows, feat = current.shape
    seqs = cell_in.shape[1]
    rows = seqs * span
    cols = heads * size
    main = (weight_q, weight_k, weight_v, weight_o)

    def loads(l):
        out = [
            pltpu.make_async_copy(w.at[l], wts.at[l, i], load_sem.at[l, i])
            for i, w in enumerate(main)
        ]
        start = pl.multiple_of(my_dp * feat, feat)
        for i, w in enumerate((weight_in, weight_forget)):
            out.append(
                pltpu.make_async_copy(
                    w.at[l, :, pl.ds(start, feat)], wgate.at[l, i], load_sem.at[l, 4 + i]
                )
            )
        out.append(pltpu.make_async_copy(cell_in.at[l], cells.at[l], load_sem.at[l, 6]))
        out.append(pltpu.make_async_copy(weight_out.at[l], wout.at[l], load_sem.at[l, 7]))
        return out

    for l in range(2):
        for copy in loads(l):
            copy.start()
    current[...] = tokens[...]

    y_size = chips if n_tp % chips == 0 else 1
    z_size = n_tp // y_size
    my_z, my_y = my_tp // y_size, lax.rem(my_tp, y_size)
    others_y = [lax.rem(my_y + j, y_size) for j in range(1, y_size)]
    others_z = [lax.rem(my_z + j, z_size) for j in range(1, z_size)]
    others_tp = [my_z * y_size + y for y in others_y] + [z * y_size + my_y for z in others_z]
    others_x = [lax.rem(my_x + j, chips) for j in range(1, chips)]
    barrier = pltpu.get_barrier_semaphore()
    for t in others_tp:
        pl.semaphore_signal(barrier, inc=1, device_id={"tp": t}, device_id_type=MESH)
    for x in others_x:
        pl.semaphore_signal(
            barrier, inc=1, device_id={"dp": x * 2 + my_core}, device_id_type=MESH
        )
    pl.semaphore_signal(barrier, inc=1, device_id={"dp": peer}, device_id_type=MESH)
    pl.semaphore_wait(barrier, len(others_tp) + chips)

    row_id = lax.broadcasted_iota(jnp.int32, (rows, rows), 0)
    col_id = lax.broadcasted_iota(jnp.int32, (rows, rows), 1)
    allowed = (row_id // span == col_id // span) & (col_id <= row_id)
    lane = lax.broadcasted_iota(jnp.int32, (rows, LANES), 1)
    row_l = lax.broadcasted_iota(jnp.int32, (rows, LANES), 0)
    reach = jnp.zeros((rows, LANES), jnp.int32)
    for b in range(seqs):
        reach = jnp.where(row_l // span == b, lengths[b], reach)
    live = lax.rem(row_l, span) < reach

    def remote(src, dst, s, r, where):
        return pltpu.make_async_remote_copy(
            src_ref=src, dst_ref=dst, send_sem=s, recv_sem=r, device_id=where, device_id_type=MESH
        )

    def tp_rows(t):
        return pl.ds(pl.multiple_of(t * own_rows, own_rows), own_rows)

    def layer(l, carry):
        def gather_z(source, target):
            return remote(
                current,
                gathered.at[l, tp_rows(source * y_size + my_y)],
                gat_s.at[l, target],
                gat_r.at[l, source],
                {"tp": target * y_size + my_y},
            )

        def gather_y(z, source, target):
            part = gathered.at[l, tp_rows(z * y_size + source)]
            return remote(
                part,
                part,
                gfw_s.at[l, z, target],
                gfw_r.at[l, z, source],
                {"tp": my_z * y_size + target},
            )

        def gather_own(source, target):
            return remote(
                current,
                gathered.at[l, tp_rows(my_z * y_size + source)],
                gfw_s.at[l, my_z, target],
                gfw_r.at[l, my_z, source],
                {"tp": my_z * y_size + target},
            )

        for z in others_z:
            gather_z(my_z, z).start()
        for y in others_y:
            gather_own(my_y, y).start()
        gathered[l, tp_rows(my_tp)] = current[...]
        incoming = loads(l)
        for copy in incoming[4:6]:
            copy.wait()
        total_heads = wgate.shape[2]
        pick_r = lax.broadcasted_iota(jnp.int32, (LANES, total_heads), 1)
        pick_c = lax.broadcasted_iota(jnp.int32, (LANES, total_heads), 0)
        head_start = my_tp * heads
        pick_in = ((pick_r == head_start + pick_c) & (pick_c < heads)).astype(F32).astype(BF16)
        pick_fg = (
            ((pick_r == head_start + pick_c - heads) & (pick_c >= heads) & (pick_c < 2 * heads))
            .astype(F32)
            .astype(BF16)
        )
        gate_w = (
            jnp.dot(pick_in, wgate[l, 0], preferred_element_type=F32)
            + jnp.dot(pick_fg, wgate[l, 1], preferred_element_type=F32)
        ).astype(BF16)
        for copy in incoming[:4]:
            copy.wait()
        for z in reversed(others_z):
            gather_z(z, z).wait_recv()
            for y in others_y:
                gather_y(z, my_y, y).start()
        for z in [my_z] + others_z:
            for y in others_y:
                gather_y(z, y, y).wait_recv()

        gain_row = gain[pl.ds(l, 1), :]
        for d in range(n_dp):
            block = gathered[l, d * rows : (d + 1) * rows].astype(F32)
            core, x = d % 2, d // 2
            scaled[core, x * rows : (x + 1) * rows] = (block * gain_row).astype(BF16)
            own_gate[core, x * rows : (x + 1) * rows] = jnp.broadcast_to(
                jnp.sum(block * block, axis=1, keepdims=True), (rows, LANES)
            )
        lane_all = lax.broadcasted_iota(jnp.int32, (chips * rows, LANES), 1)
        for core in range(2):
            part = lax.dot_general(
                scaled[core], gate_w, (((1,), (1,)), ((), ())), preferred_element_type=F32
            )
            part = jnp.where(lane_all == LANES - 3, own_gate[core], part)
            own_gate[core] = part
        send1g[...] = pack_squares(own_gate[peer_core])

        def one_gate():
            return remote(
                send1g, recv1g.at[l], one_s.at[l, 4], one_r.at[l, 4], {"dp": peer}
            )

        def one_main(c):
            return remote(
                send1.at[c], recv1.at[l, c], one_s.at[l, c], one_r.at[l, c], {"dp": peer}
            )

        def x_rows(x):
            return pl.ds(pl.multiple_of(x * rows, rows), rows)

        def two_gate(source, target):
            return remote(
                send2g.at[x_rows(target)],
                recv2g.at[l, source],
                two_s.at[l, 4, target],
                two_r.at[l, 4, source],
                {"dp": target * 2 + my_core},
            )

        def two_main(c, source, target):
            return remote(
                send2.at[c, x_rows(target)],
                recv2.at[l, c, source],
                two_s.at[l, c, target],
                two_r.at[l, c, source],
                {"dp": target * 2 + my_core},
            )

        one_gate().start()
        one_gate().wait_recv()
        both = own_gate[my_core] + recv1g[l].astype(F32)
        own_gate[my_core] = both
        send2g[...] = pack_squares(both)
        for x in others_x:
            two_gate(my_x, x).start()

        def project(c, carry):
            send1[c] = jnp.dot(
                scaled[peer_core], wts[l, c], preferred_element_type=F32
            ).astype(BF16)
            one_main(c).start()
            own = jnp.dot(scaled[my_core], wts[l, c], preferred_element_type=F32)
            one_main(c).wait_recv()
            own = own + recv1[l, c].astype(F32)
            own_main[c] = own
            send2[c] = own.astype(BF16)
            for x in others_x:
                two_main(c, my_x, x).start()
            return carry

        lax.fori_loop(0, 4, project, 0)
        incoming[6].wait()
        for x in others_x:
            two_gate(x, x).wait_recv()

        sums = own_gate[my_core, x_rows(my_x)]
        for x in others_x:
            sums = sums + recv2g[l, x].astype(F32)
        square = jnp.sum(jnp.where(lane >= LANES - 3, sums, 0.0), axis=1, keepdims=True)
        scale = lax.rsqrt(square / (feat * n_dp) + EPSILON)
        gates = scale * sums
        pad[...] = jnp.zeros_like(pad)
        pad[0:seqs, 0:heads] = max_in[l]
        pad[seqs : seqs + 1, 0:heads] = bias[pl.ds(l, 1), :]
        stabil = pad[0:seqs, :]
        forget = pltpu.roll(gates, LANES - heads, 1) + pad[seqs : seqs + 1, :]
        log_forget = jnp.minimum(forget, 0.0) - jnp.log1p(jnp.exp(-jnp.abs(forget)))
        in_gate = jnp.where(live, gates, NEG_FILL)
        log_forget = jnp.where(live, log_forget, 0.0)
        cumul = jnp.dot(
            allowed.astype(F32), log_forget, preferred_element_type=F32, precision=HIGH
        )

        def spread(value):
            wide = jnp.broadcast_to(value[:, None, :], (seqs, span, value.shape[-1]))
            return wide.reshape(rows, value.shape[-1])

        def last(value):
            return value.reshape(seqs, span, value.shape[-1])[:, span - 1, :]

        carried = cumul + spread(stabil)
        source = jnp.transpose(in_gate - cumul)

        for c in range(4):
            for x in others_x:
                two_main(c, x, x).wait_recv()
            full = own_main[c, x_rows(my_x)]
            for x in others_x:
                full = full + recv2[l, c, x].astype(F32)
            heads_buf[c] = (scale * full).astype(BF16)

        key_scale = size ** (-0.5)
        normer = norm_in[l]
        running = jnp.zeros((rows, LANES), F32)
        for h in range(heads):
            span_h = slice(h * size, (h + 1) * size)
            q, k, v = (heads_buf[c, :, span_h] for c in range(3))
            weight = jnp.where(allowed, cumul[:, h : h + 1] + source[h : h + 1, :], NEG_FILL)
            top = jnp.maximum(jnp.max(weight, axis=1, keepdims=True), carried[:, h : h + 1])
            running = jnp.where(lane == h, top, running)
            decay = jnp.exp(carried[:, h : h + 1] - top)
            scores = lax.dot_general(
                q, k, (((1,), (1,)), ((), ())), preferred_element_type=F32
            )
            scores = scores * key_scale * jnp.exp(weight - top)
            numer = jnp.dot(scores.astype(BF16), v, preferred_element_type=F32)
            from_cell = jnp.concatenate(
                [
                    jnp.dot(
                        q[b * span : (b + 1) * span],
                        cells[l, b, h].astype(BF16),
                        preferred_element_type=F32,
                    )
                    for b in range(seqs)
                ],
                axis=0,
            )
            numer = numer + decay * from_cell
            from_norm = jnp.sum(
                q.astype(F32) * spread(normer[:, h, :]), axis=1, keepdims=True
            )
            denom = jnp.sum(scores, axis=1, keepdims=True) + decay * from_norm
            readout = numer / jnp.maximum(jnp.abs(denom), 1.0)
            readout = jnp.where(live, readout, 0.0)
            outgate = heads_buf[3, :, span_h].astype(F32)
            gated[l, my_dp, :, span_h] = (readout / (1.0 + jnp.exp(-outgate))).astype(BF16)

        def across(source, target):
            return remote(
                gated.at[l, source],
                gated.at[l, source],
                gg_s.at[l, target // 2],
                gg_r.at[l, source // 2],
                {"dp": target},
            )

        def inside(block, x):
            return remote(
                gated.at[l, block], gated.at[l, block], fw_s.at[l, x], fw_r.at[l, x], {"dp": peer}
            )

        for x in others_x:
            across(my_dp, x * 2 + my_core).start()
        inside(my_dp, my_x).start()

        top_last, cumul_last = last(running), last(cumul)
        weights = jnp.exp(spread(cumul_last - top_last) - cumul + in_gate)
        fade = jnp.exp(cumul_last + stabil - top_last)
        max_out[l] = top_last[:, 0:heads]
        seq_col = lax.broadcasted_iota(jnp.int32, (size, rows), 1) // span
        pick = (
            lax.broadcasted_iota(jnp.int32, (seqs, rows), 1) // span
            == lax.broadcasted_iota(jnp.int32, (seqs, rows), 0)
        ).astype(F32)
        for h in range(heads):
            span_h = slice(h * size, (h + 1) * size)
            v = heads_buf[2, :, span_h]
            k = heads_buf[1, :, span_h].astype(F32) * key_scale * weights[:, h : h + 1]
            flipped = jnp.transpose(k)
            stacked = jnp.concatenate(
                [jnp.where(seq_col == b, flipped, 0.0).astype(BF16) for b in range(seqs)], axis=0
            )
            added = jnp.dot(stacked, v, preferred_element_type=F32)
            for b in range(seqs):
                cells[l, b, h] = (
                    fade[b : b + 1, h : h + 1] * cells[l, b, h]
                    + added[b * size : (b + 1) * size]
                )
            norm_out[l, :, h, :] = fade[:, h : h + 1] * normer[:, h, :] + jnp.dot(
                pick, k, preferred_element_type=F32, precision=HIGH
            )
        pltpu.make_async_copy(cells.at[l], cell_out.at[l], cell_sem.at[l]).start()

        for x in others_x:
            across(x * 2 + my_core, x * 2 + my_core).wait_recv()
            inside(x * 2 + my_core, x).start()
        incoming[7].wait()
        for x in [my_x] + others_x:
            inside(x * 2 + peer_core, x).wait_recv()

        def mix(d, carry):
            part = jnp.dot(gated[l, d], wout[l], preferred_element_type=F32)
            mixed[pl.ds(pl.multiple_of(d * rows, rows), rows), :] = part.astype(BF16)
            return carry

        lax.fori_loop(0, n_dp, mix, 0)

        def scatter_y(z, source, target):
            return remote(
                mixed.at[tp_rows(z * y_size + target)],
                mixed_y.at[l, z, source],
                my_s.at[l, z, target],
                my_r.at[l, z, source],
                {"tp": my_z * y_size + target},
            )

        def scatter_z(source, target):
            return remote(
                mixed_s.at[target],
                mixed_in.at[l, source],
                mix_s.at[l, target],
                mix_r.at[l, source],
                {"tp": target * y_size + my_y},
            )

        for z in others_z + [my_z]:
            for y in others_y:
                scatter_y(z, my_y, y).start()
        for z in others_z:
            gather_z(my_z, z).wait_send()
            for y in others_y:
                gather_y(z, my_y, y).wait_send()
        for y in others_y:
            gather_own(my_y, y).wait_send()
        one_gate().wait_send()
        for c in range(4):
            one_main(c).wait_send()
        for x in others_x:
            two_gate(my_x, x).wait_send()
            for c in range(4):
                two_main(c, my_x, x).wait_send()
            across(my_dp, x * 2 + my_core).wait_send()
        for x in [my_x] + others_x:
            inside(x * 2 + my_core, x).wait_send()
        for z in others_z + [my_z]:
            total = mixed[tp_rows(z * y_size + my_y), :].astype(F32)
            for y in others_y:
                scatter_y(z, y, y).wait_recv()
                total = total + mixed_y[l, z, y].astype(F32)
            if z is not my_z:
                mixed_s[z] = total.astype(BF16)
                scatter_z(my_z, z).start()
        for z in reversed(others_z):
            scatter_z(z, z).wait_recv()
            total = total + mixed_in[l, z].astype(F32)
        current[...] = (current[...].astype(F32) + total).astype(BF16)
        for z in others_z:
            scatter_z(my_z, z).wait_send()
        for z in others_z + [my_z]:
            for y in others_y:
                scatter_y(z, my_y, y).wait_send()
        return carry

    lax.fori_loop(0, 2, layer, 0)
    tokens_out[...] = current[...]
    for l in range(2):
        pltpu.make_async_copy(cells.at[l], cell_out.at[l], cell_sem.at[l]).wait()


def per_device(
    tokens,
    lengths,
    norm_gain,
    query_weight,
    key_weight,
    value_weight,
    outgate_weight,
    input_gate_weight,
    forget_gate_weight,
    forget_bias,
    out_weight,
    cell_state,
    norm_state,
    max_state,
):
    n_tp, n_dp = lax.axis_size("tp"), lax.axis_size("dp")
    seq_here, span, feat = tokens.shape
    seqs, heads, size = cell_state.shape[1:4]
    own_rows, rows, cols, chips = seq_here * span, seqs * span, heads * size, n_dp // 2
    everyone = n_tp * own_rows
    n_y = chips if n_tp % chips == 0 else 1
    n_z = n_tp // n_y
    vmem = pl.BlockSpec(memory_space=pltpu.VMEM)
    smem = pl.BlockSpec(memory_space=pltpu.SMEM)
    hbm = pl.BlockSpec(memory_space=pl.ANY)
    V, sem = pltpu.VMEM, pltpu.SemaphoreType.DMA
    result = pl.pallas_call(
        functools.partial(kernel, (n_tp, n_dp, span, heads, size)),
        out_shape=(
            jax.ShapeDtypeStruct((own_rows, feat), BF16),
            jax.ShapeDtypeStruct(cell_state.shape, F32),
            jax.ShapeDtypeStruct(norm_state.shape, F32),
            jax.ShapeDtypeStruct(max_state.shape, F32),
        ),
        in_specs=[smem, vmem, vmem, hbm, hbm, hbm, hbm, hbm, hbm, vmem, hbm, hbm, vmem, vmem],
        out_specs=(vmem, hbm, vmem, vmem),
        scratch_shapes=[
            V((own_rows, feat), BF16),
            V((2, 4, feat, cols), BF16),
            V((2, 2, input_gate_weight.shape[2], feat), BF16),
            V((2, cols, feat), BF16),
            V(cell_state.shape, F32),
            V((seqs + 8, LANES), F32),
            V((2, everyone, feat), BF16),
            V((2, chips * rows, feat), BF16),
            V((4, chips * rows, cols), F32),
            V((2, chips * rows, LANES), F32),
            V((4, chips * rows, cols), BF16),
            V((chips * rows, LANES), BF16),
            V((2, 4, chips * rows, cols), BF16),
            V((2, chips * rows, LANES), BF16),
            V((4, chips * rows, cols), BF16),
            V((chips * rows, LANES), BF16),
            V((2, 4, chips, rows, cols), BF16),
            V((2, chips, rows, LANES), BF16),
            V((4, rows, cols), BF16),
            V((2, n_dp, rows, cols), BF16),
            V((everyone, feat), BF16),
            V((n_z, own_rows, feat), BF16),
            V((2, n_z, n_y, own_rows, feat), BF16),
            V((2, n_z, own_rows, feat), BF16),
            sem((2, 8)),
            sem((2,)),
            sem((2, n_z)),
            sem((2, n_z)),
            sem((2, n_z, n_y)),
            sem((2, n_z, n_y)),
            sem((2, 5)),
            sem((2, 5)),
            sem((2, 5, chips)),
            sem((2, 5, chips)),
            sem((2, chips)),
            sem((2, chips)),
            sem((2, chips)),
            sem((2, chips)),
            sem((2, n_z)),
            sem((2, n_z)),
            sem((2, n_z, n_y)),
            sem((2, n_z, n_y)),
        ],
        compiler_params=pltpu.CompilerParams(
            collective_id=0, has_side_effects=True, vmem_limit_bytes=60 * 1024 * 1024
        ),
    )(
        lengths,
        tokens.reshape(own_rows, feat),
        norm_gain,
        query_weight,
        key_weight,
        value_weight,
        outgate_weight,
        jnp.swapaxes(input_gate_weight, 1, 2),
        jnp.swapaxes(forget_gate_weight, 1, 2),
        forget_bias,
        out_weight,
        cell_state,
        norm_state,
        max_state,
    )
    return (result[0].reshape(tokens.shape), *result[1:])


def solution(mesh):
    return jax.shard_map(
        per_device,
        mesh=mesh,
        in_specs=(
            P("tp", None, "dp"),
            P("dp"),
            P(None, "dp"),
            P(None, "dp", "tp"),
            P(None, "dp", "tp"),
            P(None, "dp", "tp"),
            P(None, "dp", "tp"),
            P(),
            P(),
            P(None, "tp"),
            P(None, "tp", "dp"),
            P(None, "dp", "tp", None, None),
            P(None, "dp", "tp", None),
            P(None, "dp", "tp"),
        ),
        out_specs=(
            P("tp", None, "dp"),
            P(None, "dp", "tp", None, None),
            P(None, "dp", "tp", None),
            P(None, "dp", "tp"),
        ),
        check_vma=False,
    )
```

profile of v0, /device:TPU:0, one launch (start us, length us, event | category | flops | bytes accessed | tf_op | source)
XLA Modules:
  0.0 143.9 jit_solution(1372726705314823351)
XLA Ops:
  0.6 1.4 copy.18.max_in
  2.0 133.6 %shard_map.165 = (bf16[64,1024]{1,0:T(8,128)(2,1)}, f32[2,8,4,128,128]{4,3,2,1,0:T(8,128)}, f32[2,8,4,128]{3,2,1,0:T(4,128)}, f32[2,8,4]{2,1,0:T(8,128)}) custom-call(s32[8]{0:T(128)} %lengths.1, bf16[64,1024]{1,0:T(8,128)(2,1)} %bitcast.6, f32[2,1024]{1,0:T(2,128)} %gain.1, bf16[2,1024,512]{2,1,0:T(8,128)(2,1)} %weight_q.1, bf16[2,1024,512]{2,1,0:T(8,128)(2,1)} %weight_k.1, ...), custom_call_target="tpu_custom_call" | custom-call | tf_op jit(solution)/shard_map/pallas_call | solution.py:518
  135.6 1.4 copy.19
  137.0 1.6 %copy.23 = bf16[4,16,1024]{2,1,0:T(8,128)(2,1)} copy(bf16[4,16,1024]{2,1,0:T(8,128)(2,1)} %bitcast.7) | data formatting | bytes 262144
  138.5 0.0 copy-start
  138.5 4.7 %copy.24 = f32[2,8,4,128,128]{4,3,2,1,0:T(8,128)} copy(f32[2,8,4,128,128]{4,3,2,1,0:T(8,128)} %get-tuple-element.21) | data formatting | bytes 8388608
  143.3 0.0 copy-done
  143.3 0.6 copy.25
Async XLA Ops:
  138.5 4.7 %copy-start = (f32[2,8,4,128]{3,2,1,0:T(4,128)S(1)}, f32[2,8,4,128]{3,2,1,0:T(4,128)}, u32[]{:S(2)}) copy-start(f32[2,8,4,128]{3,2,1,0:T(4,128)} %get-tuple-element.22) | copy-start | bytes 98308
where the time goes:
time: 145 us; the launch traced here: 144 us
  Pallas kernels  134 us (92%)
  local copies, waits for them, and re-layouts  9.62 us (7%)
    pallas_call x1, Pallas kernels, per_device(): pl.pallas_call(functools.partial(kernel, (n_tp, n_dp, span, heads, size))...  134 us
    unnamed x7, local copies, waits for them, and re-layouts  9.62 us

commit v1 on v0

--- a/solution.py
+++ b/solution.py
@@ -44,14 +44,13 @@
     norm_in,
     max_in,
     tokens_out,
-    cell_out,
+    cells,
     norm_out,
     max_out,
     current,
     wts,
     wgate,
     wout,
-    cells,
     pad,
     gathered,
     scaled,
@@ -72,7 +71,6 @@
     mixed_y,
     mixed_in,
     load_sem,
-    cell_sem,
     gat_s,
     gat_r,
     gfw_s,
@@ -301,7 +299,7 @@
         scale = lax.rsqrt(square / (feat * n_dp) + EPSILON)
         gates = scale * sums
         pad[...] = jnp.zeros_like(pad)
-        pad[0:seqs, 0:heads] = max_in[l]
+        pad[0:seqs, 0:heads] = jnp.transpose(max_in[l])
         pad[seqs : seqs + 1, 0:heads] = bias[pl.ds(l, 1), :]
         stabil = pad[0:seqs, :]
         forget = pltpu.roll(gates, LANES - heads, 1) + pad[seqs : seqs + 1, :]
@@ -387,7 +385,7 @@
         top_last, cumul_last = last(running), last(cumul)
         weights = jnp.exp(spread(cumul_last - top_last) - cumul + in_gate)
         fade = jnp.exp(cumul_last + stabil - top_last)
-        max_out[l] = top_last[:, 0:heads]
+        max_out[l] = jnp.transpose(top_last)[0:heads, :]
         seq_col = lax.broadcasted_iota(jnp.int32, (size, rows), 1) // span
         pick = (
             lax.broadcasted_iota(jnp.int32, (seqs, rows), 1) // span
@@ -410,7 +408,6 @@
             norm_out[l, :, h, :] = fade[:, h : h + 1] * normer[:, h, :] + jnp.dot(
                 pick, k, preferred_element_type=F32, precision=HIGH
             )
-        pltpu.make_async_copy(cells.at[l], cell_out.at[l], cell_sem.at[l]).start()
 
         for x in others_x:
             across(x * 2 + my_core, x * 2 + my_core).wait_recv()
@@ -484,8 +481,15 @@
 
     lax.fori_loop(0, 2, layer, 0)
     tokens_out[...] = current[...]
-    for l in range(2):
-        pltpu.make_async_copy(cells.at[l], cell_out.at[l], cell_sem.at[l]).wait()
+
+
+def store(*refs):
+    sem = refs[-1]
+    copies = [pltpu.make_async_copy(refs[i], refs[4 + i], sem.at[i]) for i in range(4)]
+    for copy in copies:
+        copy.start()
+    for copy in copies:
+        copy.wait()
 
 
 def per_device(
@@ -518,19 +522,18 @@
     result = pl.pallas_call(
         functools.partial(kernel, (n_tp, n_dp, span, heads, size)),
         out_shape=(
-            jax.ShapeDtypeStruct((own_rows, feat), BF16),
-            jax.ShapeDtypeStruct(cell_state.shape, F32),
-            jax.ShapeDtypeStruct(norm_state.shape, F32),
-            jax.ShapeDtypeStruct(max_state.shape, F32),
+            V((own_rows, feat), BF16),
+            V(cell_state.shape, F32),
+            V(norm_state.shape, F32),
+            V((2, heads, seqs), F32),
         ),
         in_specs=[smem, vmem, vmem, hbm, hbm, hbm, hbm, hbm, hbm, vmem, hbm, hbm, vmem, vmem],
-        out_specs=(vmem, hbm, vmem, vmem),
+        out_specs=(vmem, vmem, vmem, vmem),
         scratch_shapes=[
             V((own_rows, feat), BF16),
             V((2, 4, feat, cols), BF16),
             V((2, 2, input_gate_weight.shape[2], feat), BF16),
             V((2, cols, feat), BF16),
-            V(cell_state.shape, F32),
             V((seqs + 8, LANES), F32),
             V((2, everyone, feat), BF16),
             V((2, chips * rows, feat), BF16),
@@ -551,7 +554,6 @@
             V((2, n_z, n_y, own_rows, feat), BF16),
             V((2, n_z, own_rows, feat), BF16),
             sem((2, 8)),
-            sem((2,)),
             sem((2, n_z)),
             sem((2, n_z)),
             sem((2, n_z, n_y)),
@@ -570,7 +572,7 @@
             sem((2, n_z, n_y)),
         ],
         compiler_params=pltpu.CompilerParams(
-            collective_id=0, has_side_effects=True, vmem_limit_bytes=60 * 1024 * 1024
+            collective_id=0, has_side_effects=True, vmem_limit_bytes=48 * 1024 * 1024
         ),
     )(
         lengths,
@@ -586,9 +588,17 @@
         out_weight,
         cell_state,
         norm_state,
-        max_state,
+        jnp.swapaxes(max_state, 1, 2),
     )
-    return (result[0].reshape(tokens.shape), *result[1:])
+    result = pl.pallas_call(
+        store,
+        out_shape=tuple(jax.ShapeDtypeStruct(part.shape, part.dtype) for part in result),
+        in_specs=[vmem] * 4,
+        out_specs=(hbm,) * 4,
+        scratch_shapes=[sem((4,))],
+        compiler_params=pltpu.CompilerParams(vmem_limit_bytes=16 * 1024 * 1024),
+    )(*result)
+    return (result[0].reshape(tokens.shape), *result[1:3], jnp.swapaxes(result[3], 1, 2))
 
 
 def solution(mesh):

time: 145 us -> 143 us (0.986)
  local copies, waits for them, and re-layouts: 9.62 us -> 6.45 us
    unnamed x7 -> x16, local copies, waits for them, and re-layouts: 9.62 us -> 6.45 us
    pallas_call x0 -> x1, Pallas kernels: none -> 2.1 us  [per_device(): pl.pallas_call(store, out_shape=tuple((jax.ShapeDtypeStruct(part.shape, p...]
where the time goes in v1:
time: 143 us; the launch traced here: 142 us
  Pallas kernels  135 us (94%)
  local copies, waits for them, and re-layouts  6.45 us (5%)
    pallas_call x1, Pallas kernels, per_device(): pl.pallas_call(functools.partial(kernel, (n_tp, n_dp, span, heads, size))...  133 us
    unnamed x16, local copies, waits for them, and re-layouts  6.45 us

profile of v1, /device:TPU:0, one launch (start us, length us, event | category | flops | bytes accessed | tf_op | source)
XLA Modules:
  0.0 141.8 jit_solution(6987064980922080618)
XLA Ops:
  0.6 0.0 copy-start
  0.6 1.0 copy-done
  1.7 0.0 copy-start.1
  1.7 1.0 copy-done.1
  2.7 0.0 copy-start.2
  2.7 0.9 copy-done.2
  3.6 0.0 copy-start.3
  3.6 0.8 copy-done.3
  4.4 0.0 copy-start.4
  4.4 0.7 copy-done.4
  5.1 0.0 copy-start.5
  5.1 0.7 copy-done.5
  5.8 0.0 copy-start.6
  5.8 0.7 copy-done.6
  6.4 0.0 copy-start.7
  6.5 0.7 copy-done.7
  7.1 132.6 %shard_map.165 = (bf16[64,1024]{1,0:T(8,128)(2,1)S(1)}, f32[2,8,4,128,128]{4,3,2,1,0:T(8,128)S(1)}, f32[2,8,4,128]{3,2,1,0:T(4,128)S(1)}, f32[2,4,8]{2,1,0:T(4,128)S(1)}) custom-call(s32[8]{0:T(128)S(1)} %copy-done.7, bf16[64,1024]{1,0:T(8,128)(2,1)S(1)} %bitcast.8, f32[2,1024]{1,0:T(2,128)S(1)} %copy-done.4, bf16[2,1024,512]{2,1,0:T(8,128)(2,1)} %weight_q.1, ...), custom_call_target="tpu_custom_call" | custom-call | tf_op jit(solution)/shard_map/pallas_call | solution.py:522
  139.7 2.1 %shard_map.166 = (bf16[64,1024]{1,0:T(8,128)(2,1)}, f32[2,8,4,128,128]{4,3,2,1,0:T(8,128)}, f32[2,8,4,128]{3,2,1,0:T(4,128)}, f32[2,4,8]{2,1,0:T(4,128)}) custom-call(bf16[64,1024]{1,0:T(8,128)(2,1)S(1)} %get-tuple-element.12.refs_0_, f32[2,8,4,128,128]{4,3,2,1,0:T(8,128)S(1)} %get-tuple-element.13.refs_1_, f32[2,8,4,128]{3,2,1,0:T(4,128)S(1)} %get-tuple-element.14.refs_2_, ...), custom_call_target="tpu_custom_call" | custom-call | tf_op jit(solution)/shard_map/pallas_call | solution.py:593
Async XLA Ops:
  0.6 1.0 copy-start
  1.7 1.0 copy-start.1
  2.7 0.9 copy-start.2
  3.6 0.8 copy-start.3
  4.4 0.7 copy-start.4
  5.1 0.7 copy-start.5
  5.8 0.7 copy-start.6
  6.4 0.7 copy-start.7

commit v2 on v1

v2 whole, which is shorter than its diff:
```python
import functools
import jax
import jax.numpy as jnp
from jax import lax
from jax.experimental import pallas as pl
from jax.experimental.pallas import tpu as pltpu
from jax.sharding import PartitionSpec as P

EPSILON = 1e-06
NEG_FILL = -1e30
LANES = 128
HIGH = lax.Precision.HIGHEST
BF16 = jnp.bfloat16
F32 = jnp.float32
MESH = pl.DeviceIdType.MESH
BATCHES = 2
LAYERS = 2
ISSUE = {
    "forward": 3.0,
    "project": 12.0,
    "exchange": 12.1,
    "attend": 21.0,
    "relay": 25.0,
    "mix": 28.0,
    "fold": 31.0,
    "finish": 40.0,
}
LAG = 5.6
PERIOD = 40.5


def pack_squares(block):
    lane = lax.broadcasted_iota(jnp.int32, block.shape, 1)
    square = jnp.sum(jnp.where(lane >= LANES - 3, block, 0.0), axis=1, keepdims=True)
    first = square.astype(BF16).astype(F32)
    rest = square - first
    second = rest.astype(BF16).astype(F32)
    third = rest - second
    block = jnp.where(lane == LANES - 3, first, block)
    block = jnp.where(lane == LANES - 2, second, block)
    return jnp.where(lane == LANES - 1, third, block).astype(BF16)


def flip_bits(value, mask):
    result = value
    bit = 1
    while bit <= mask:
        if mask & bit:
            result = result + bit * (1 - 2 * lax.rem(value // bit, 2))
        bit = bit * 2
    return result


def kernel(sizes, *refs):
    n_tp, n_dp, span, heads, size, n_y, names = sizes
    r = dict(zip(names, refs))
    lengths, norm, stabils, gain = r["lengths"], r["norm"], r["stabils"], r["gain"]
    cells, norm_out, max_out, tokens_out = r["cells"], r["norm_out"], r["max_out"], r["tokens_out"]
    current, wts, wgate, wout = r["current"], r["wts"], r["wgate"], r["wout"]
    gathered, scaled, gate_w, both = r["gathered"], r["scaled"], r["gate_w"], r["both"]
    own_gate, own_main, heads_buf = r["own_gate"], r["own_main"], r["heads_buf"]
    gated, mixed, top_buf, pad = r["gated"], r["mixed"], r["top_buf"], r["pad"]
    load_sem = r["load_sem"]
    chips = n_dp // 2
    n_z = n_tp // n_y
    my_tp, my_dp = lax.axis_index("tp"), lax.axis_index("dp")
    my_x, my_core = my_dp // 2, lax.rem(my_dp, 2)
    peer_core = 1 - my_core
    peer = my_x * 2 + peer_core
    my_z, my_y = my_tp // n_y, lax.rem(my_tp, n_y)
    own_rows, feat = current.shape[2:]
    seqs = cells.shape[1]
    own_part = own_rows // span
    own_seqs = own_part * BATCHES
    ratio = seqs // own_seqs
    seqs_b = seqs // BATCHES
    rows = seqs_b * span
    total_rows = n_dp * rows
    key_scale = size ** (-0.5)

    def load(index, source, target):
        return pltpu.make_async_copy(source, target, load_sem.at[index])

    start = pl.multiple_of(my_dp * feat, feat)
    small = [
        load(0, r["tokens"], current.at[0]),
        load(1, r["lengths_in"], lengths),
        load(2, r["gain_in"], gain),
        load(3, r["norm_in"], norm),
        load(4, r["max_in"], stabils),
        load(5, r["bias_in"], r["bias"]),
    ]
    big = []
    for l in range(LAYERS):
        part = []
        for i, name in enumerate(("weight_in", "weight_forget")):
            part.append(load(6 + 8 * l + i, r[name].at[l, :, pl.ds(start, feat)], wgate.at[l, i]))
        for i, name in enumerate(("weight_q", "weight_k", "weight_v", "weight_o")):
            part.append(load(8 + 8 * l + i, r[name].at[l], wts.at[l, i]))
        part.append(load(12 + 8 * l, r["cell_in"].at[l], cells.at[l]))
        part.append(load(13 + 8 * l, r["weight_out"].at[l], wout.at[l]))
        big.append(part)
    for copy in small + big[0] + big[1]:
        copy.start()

    others_y = [lax.rem(my_y + j, n_y) for j in range(1, n_y)]
    power = n_z & (n_z - 1) == 0
    others_z = [flip_bits(my_z, j) if power else lax.rem(my_z + j, n_z) for j in range(1, n_z)]
    sources_z = others_z if power else [lax.rem(my_z + n_z - j, n_z) for j in range(1, n_z)]
    others_tp = [my_z * n_y + y for y in others_y] + [z * n_y + my_y for z in others_z]
    others_x = [lax.rem(my_x + j, chips) for j in range(1, chips)]
    barrier = pltpu.get_barrier_semaphore()
    for t in others_tp:
        pl.semaphore_signal(barrier, inc=1, device_id={"tp": t}, device_id_type=MESH)
    for x in others_x:
        pl.semaphore_signal(
            barrier, inc=1, device_id={"dp": x * 2 + my_core}, device_id_type=MESH
        )
    pl.semaphore_signal(barrier, inc=1, device_id={"dp": peer}, device_id_type=MESH)
    pl.semaphore_wait(barrier, len(others_tp) + chips)

    def remote(src, dst, s, rcv, where):
        return pltpu.make_async_remote_copy(
            src_ref=src, dst_ref=dst, send_sem=s, recv_sem=rcv, device_id=where, device_id_type=MESH
        )

    def tp_rows(t):
        return pl.ds(pl.multiple_of(t * own_rows, own_rows), own_rows)

    def x_rows(x):
        return pl.ds(pl.multiple_of(x * rows, rows), rows)

    def gather_z(l, b, source, target):
        return remote(
            current.at[l, b],
            gathered.at[l, b, tp_rows(source * n_y + my_y)],
            r["gat_s"].at[l, b, target],
            r["gat_r"].at[l, b, source],
            {"tp": target * n_y + my_y},
        )

    def gather_y(l, b, z, source, target, own=False):
        part = gathered.at[l, b, tp_rows(z * n_y + source)]
        return remote(
            current.at[l, b] if own else part,
            part,
            r["gfw_s"].at[l, b, z, target],
            r["gfw_r"].at[l, b, z, source],
            {"tp": my_z * n_y + target},
        )

    def one_gate(l, b):
        return remote(
            r["send1g"].at[l, b],
            r["recv1g"].at[l, b],
            r["one_s"].at[l, b, 4],
            r["one_r"].at[l, b, 4],
            {"dp": peer},
        )

    def one_main(l, b, c):
        return remote(
            r["send1"].at[l, b, c],
            r["recv1"].at[l, b, c],
            r["one_s"].at[l, b, c],
            r["one_r"].at[l, b, c],
            {"dp": peer},
        )

    def two_gate(l, b, source, target):
        return remote(
            r["send2g"].at[l, b, x_rows(target)],
            r["recv2g"].at[l, b, source],
            r["two_s"].at[l, b, 4, target],
            r["two_r"].at[l, b, 4, source],
            {"dp": target * 2 + my_core},
        )

    def two_main(l, b, c, source, target):
        return remote(
            r["send2"].at[l, b, c, x_rows(target)],
            r["recv2"].at[l, b, c, source],
            r["two_s"].at[l, b, c, target],
            r["two_r"].at[l, b, c, source],
            {"dp": target * 2 + my_core},
        )

    def across(l, b, source, target):
        return remote(
            gated.at[l, b, source],
            gated.at[l, b, source],
            r["gg_s"].at[l, b, target // 2],
            r["gg_r"].at[l, b, source // 2],
            {"dp": target},
        )

    def inside(l, b, block, x):
        return remote(
            gated.at[l, b, block],
            gated.at[l, b, block],
            r["fw_s"].at[l, b, x],
            r["fw_r"].at[l, b, x],
            {"dp": peer},
        )

    def scatter_y(l, b, z, source, target):
        return remote(
            mixed.at[l, b, tp_rows(z * n_y + target)],
            r["mixed_y"].at[l, b, z, source],
            r["my_s"].at[l, b, z, target],
            r["my_r"].at[l, b, z, source],
            {"tp": my_z * n_y + target},
        )

    def scatter_z(l, b, source, target):
        return remote(
            r["mixed_s"].at[l, b, target],
            r["mixed_in"].at[l, b, source],
            r["mix_s"].at[l, b, target],
            r["mix_r"].at[l, b, source],
            {"tp": target * n_y + my_y},
        )

    def begin(l, b):
        for z in others_z:
            gather_z(l, b, my_z, z).start()
        for y in others_y:
            gather_y(l, b, my_z, my_y, y, own=True).start()
        gathered[l, b, tp_rows(my_tp)] = current[l, b]

    small[0].wait()
    for b in range(BATCHES):
        begin(0, b)
    for copy in small[1:]:
        copy.wait()

    row_id = lax.broadcasted_iota(jnp.int32, (rows, rows), 0)
    col_id = lax.broadcasted_iota(jnp.int32, (rows, rows), 1)
    allowed = (row_id // span == col_id // span) & (col_id <= row_id)
    lane = lax.broadcasted_iota(jnp.int32, (rows, LANES), 1)
    row_l = lax.broadcasted_iota(jnp.int32, (rows, LANES), 0)
    runs = [
        [slice(j * own_seqs + b * own_part, j * own_seqs + (b + 1) * own_part) for j in range(ratio)]
        for b in range(BATCHES)
    ]

    def live_of(b):
        reach = jnp.zeros((rows, LANES), jnp.int32)
        place = 0
        for run in runs[b]:
            for s in range(run.start, run.stop):
                reach = jnp.where(row_l // span == place, lengths[s], reach)
                place = place + 1
        return lax.rem(row_l, span) < reach

    pad[...] = jnp.zeros_like(pad)
    for l in range(LAYERS):
        pad[l, 0:seqs, 0:heads] = jnp.transpose(stabils[l])
        pad[l, seqs : seqs + 1, 0:heads] = r["bias"][l : l + 1, :]

    def spread(value):
        wide = jnp.broadcast_to(value[:, None, :], (seqs_b, span, value.shape[-1]))
        return wide.reshape(rows, value.shape[-1])

    def last(value):
        return value.reshape(seqs_b, span, value.shape[-1])[:, span - 1, :]

    def gate_columns(l):
        for copy in big[l][:2]:
            copy.wait()
        total_heads = wgate.shape[2]
        pick_r = lax.broadcasted_iota(jnp.int32, (LANES, total_heads), 1)
        pick_c = lax.broadcasted_iota(jnp.int32, (LANES, total_heads), 0)
        head_start = my_tp * heads
        pick_in = ((pick_r == head_start + pick_c) & (pick_c < heads)).astype(F32).astype(BF16)
        pick_fg = (
            ((pick_r == head_start + pick_c - heads) & (pick_c >= heads) & (pick_c < 2 * heads))
            .astype(F32)
            .astype(BF16)
        )
        gate_w[l] = (
            jnp.dot(pick_in, wgate[l, 0], preferred_element_type=F32)
            + jnp.dot(pick_fg, wgate[l, 1], preferred_element_type=F32)
        ).astype(BF16)

    for l in range(LAYERS):
        gate_columns(l)

    def forward(l, b, j):
        z = sources_z[j]
        gather_z(l, b, z, z).wait_recv()
        for y in others_y:
            gather_y(l, b, z, my_y, y).start()

    def project(l, b):
        for z in [my_z] + others_z:
            for y in others_y:
                gather_y(l, b, z, y, y).wait_recv()
        gain_row = gain[l : l + 1, :]
        for d in range(n_dp):
            block = gathered[l, b, d * rows : (d + 1) * rows].astype(F32)
            core, x = d % 2, d // 2
            scaled[core, x * rows : (x + 1) * rows] = (block * gain_row).astype(BF16)
            own_gate[b, core, x * rows : (x + 1) * rows] = jnp.broadcast_to(
                jnp.sum(block * block, axis=1, keepdims=True), (rows, LANES)
            )
        lane_all = lax.broadcasted_iota(jnp.int32, (chips * rows, LANES), 1)
        for core in range(2):
            part = lax.dot_general(
                scaled[core], gate_w[l], (((1,), (1,)), ((), ())), preferred_element_type=F32
            )
            own_gate[b, core] = jnp.where(lane_all == LANES - 3, own_gate[b, core], part)
        r["send1g"][l, b] = pack_squares(own_gate[b, peer_core])
        one_gate(l, b).start()
        if b == 0:
            for copy in big[l][2:6]:
                copy.wait()

        def one(c, carry):
            flat = scaled[...].reshape(2 * chips * rows, feat)
            both[...] = jnp.dot(flat, wts[l, c], preferred_element_type=F32).reshape(both.shape)
            r["send1"][l, b, c] = both[peer_core].astype(BF16)
            one_main(l, b, c).start()
            own_main[b, c] = both[my_core]
            return carry

        lax.fori_loop(0, 4, one, 0)

    def exchange(l, b):
        one_gate(l, b).wait_recv()
        summed = own_gate[b, my_core] + r["recv1g"][l, b].astype(F32)
        own_gate[b, my_core] = summed
        r["send2g"][l, b] = pack_squares(summed)
        for x in others_x:
            two_gate(l, b, my_x, x).start()

        def one(c, carry):
            one_main(l, b, c).wait_recv()
            own = own_main[b, c] + r["recv1"][l, b, c].astype(F32)
            own_main[b, c] = own
            r["send2"][l, b, c] = own.astype(BF16)
            for x in others_x:
                two_main(l, b, c, my_x, x).start()
            return carry

        lax.fori_loop(0, 4, one, 0)

    def attend(l, b):
        live = live_of(b)
        for x in others_x:
            two_gate(l, b, x, x).wait_recv()
        sums = own_gate[b, my_core, x_rows(my_x)]
        for x in others_x:
            sums = sums + r["recv2g"][l, b, x].astype(F32)
        square = jnp.sum(jnp.where(lane >= LANES - 3, sums, 0.0), axis=1, keepdims=True)
        scale = lax.rsqrt(square / (feat * n_dp) + EPSILON)
        gates = scale * sums
        stabil = jnp.concatenate([pad[l, run] for run in runs[b]], axis=0)
        forget = pltpu.roll(gates, LANES - heads, 1) + pad[l, seqs : seqs + 1, :]
        log_forget = jnp.minimum(forget, 0.0) - jnp.log1p(jnp.exp(-jnp.abs(forget)))
        in_gate = jnp.where(live, gates, NEG_FILL)
        log_forget = jnp.where(live, log_forget, 0.0)
        cumul = jnp.dot(
            allowed.astype(F32), log_forget, preferred_element_type=F32, precision=HIGH
        )
        carried = cumul + spread(stabil)
        source = jnp.transpose(in_gate - cumul)
        if b == 0:
            big[l][6].wait()
        for c in range(4):
            for x in others_x:
                two_main(l, b, c, x, x).wait_recv()
            full = own_main[b, c, x_rows(my_x)]
            for x in others_x:
                full = full + r["recv2"][l, b, c, x].astype(F32)
            heads_buf[b, c] = (scale * full).astype(BF16)

        ids = [s for run in runs[b] for s in range(run.start, run.stop)]
        running = jnp.zeros((rows, LANES), F32)
        for h in range(heads):
            span_h = slice(h * size, (h + 1) * size)
            normer = jnp.concatenate([norm[l, run, h, :] for run in runs[b]], axis=0)
            q, k, v = (heads_buf[b, c, :, span_h] for c in range(3))
            weight = jnp.where(allowed, cumul[:, h : h + 1] + source[h : h + 1, :], NEG_FILL)
            top = jnp.maximum(jnp.max(weight, axis=1, keepdims=True), carried[:, h : h + 1])
            running = jnp.where(lane == h, top, running)
            decay = jnp.exp(carried[:, h : h + 1] - top)
            scores = lax.dot_general(
                q, k, (((1,), (1,)), ((), ())), preferred_element_type=F32
            )
            scores = scores * key_scale * jnp.exp(weight - top)
            numer = jnp.dot(scores.astype(BF16), v, preferred_element_type=F32)
            from_cell = jnp.concatenate(
                [
                    jnp.dot(
                        q[i * span : (i + 1) * span],
                        cells[l, s, h].astype(BF16),
                        preferred_element_type=F32,
                    )
                    for i, s in enumerate(ids)
                ],
                axis=0,
            )
            numer = numer + decay * from_cell
            from_norm = jnp.sum(q.astype(F32) * spread(normer), axis=1, keepdims=True)
            denom = jnp.sum(scores, axis=1, keepdims=True) + decay * from_norm
            readout = numer / jnp.maximum(jnp.abs(denom), 1.0)
            readout = jnp.where(live, readout, 0.0)
            outgate = heads_buf[b, 3, :, span_h].astype(F32)
            gated[l, b, my_dp, :, span_h] = (readout / (1.0 + jnp.exp(-outgate))).astype(BF16)

        for x in others_x:
            across(l, b, my_dp, x * 2 + my_core).start()
        inside(l, b, my_dp, my_x).start()

        top_last, cumul_last = last(running), last(cumul)
        weights = jnp.exp(spread(cumul_last - top_last) - cumul + in_gate)
        fade = jnp.exp(cumul_last + stabil - top_last)
        for j, run in enumerate(runs[b]):
            top_buf[l, run] = top_last[j * own_part : (j + 1) * own_part]
        seq_col = lax.broadcasted_iota(jnp.int32, (size, rows), 1) // span
        pick = (
            lax.broadcasted_iota(jnp.int32, (seqs_b, rows), 1) // span
            == lax.broadcasted_iota(jnp.int32, (seqs_b, rows), 0)
        ).astype(F32)
        for h in range(heads):
            span_h = slice(h * size, (h + 1) * size)
            normer = jnp.concatenate([norm[l, run, h, :] for run in runs[b]], axis=0)
            v = heads_buf[b, 2, :, span_h]
            k = heads_buf[b, 1, :, span_h].astype(F32) * key_scale * weights[:, h : h + 1]
            flipped = jnp.transpose(k)
            stacked = jnp.concatenate(
                [jnp.where(seq_col == i, flipped, 0.0).astype(BF16) for i in range(seqs_b)], axis=0
            )
            added = jnp.dot(stacked, v, preferred_element_type=F32)
            for i, s in enumerate(ids):
                cells[l, s, h] = (
                    fade[i : i + 1, h : h + 1] * cells[l, s, h]
                    + added[i * size : (i + 1) * size]
                )
            moved = fade[:, h : h + 1] * normer + jnp.dot(
                pick, k, preferred_element_type=F32, precision=HIGH
            )
            for j, run in enumerate(runs[b]):
                norm_out[l, run, h, :] = moved[j * own_part : (j + 1) * own_part]

    def relay(l, b):
        for x in others_x:
            across(l, b, x * 2 + my_core, x * 2 + my_core).wait_recv()
            inside(l, b, x * 2 + my_core, x).start()

    def mix(l, b):
        if b == 0:
            big[l][7].wait()
        for x in [my_x] + others_x:
            inside(l, b, x * 2 + peer_core, x).wait_recv()
        flat = gated[l, b].reshape(total_rows, heads * size)
        mixed[l, b] = jnp.dot(flat, wout[l], preferred_element_type=F32).astype(BF16)
        for z in others_z[::-1] + [my_z]:
            for y in others_y:
                scatter_y(l, b, z, my_y, y).start()

    def folded(l, b, z):
        total = mixed[l, b, tp_rows(z * n_y + my_y), :].astype(F32)
        for y in others_y:
            scatter_y(l, b, z, y, y).wait_recv()
            total = total + r["mixed_y"][l, b, z, y].astype(F32)
        return total

    def fold(l, b):
        for z in others_z[::-1]:
            r["mixed_s"][l, b, z] = folded(l, b, z).astype(BF16)
            scatter_z(l, b, my_z, z).start()

    def finish(l, b):
        total = folded(l, b, my_z)
        for z in sources_z:
            scatter_z(l, b, z, z).wait_recv()
            total = total + r["mixed_in"][l, b, z].astype(F32)
        result = (current[l, b].astype(F32) + total).astype(BF16)
        if l == LAYERS - 1:
            tokens_out[b] = result
        else:
            current[l + 1, b] = result
            begin(l + 1, b)

    steps = []
    for l in range(LAYERS):
        for b in range(BATCHES):
            base = l * PERIOD + b * LAG
            for j in range(n_z - 1):
                steps.append((base + ISSUE["forward"] * (j + 1), functools.partial(forward, l, b, j)))
            for name, step in (
                ("project", project),
                ("exchange", exchange),
                ("attend", attend),
                ("relay", relay),
                ("mix", mix),
                ("fold", fold),
                ("finish", finish),
            ):
                steps.append((base + ISSUE[name], functools.partial(step, l, b)))
    for _, step in sorted(steps, key=lambda item: item[0]):
        step()

    for l in range(LAYERS):
        max_out[l] = jnp.transpose(top_buf[l])[0:heads, :]
    for l in range(LAYERS):
        for b in range(BATCHES):
            for z in others_z:
                gather_z(l, b, my_z, z).wait_send()
                scatter_z(l, b, my_z, z).wait_send()
                for y in others_y:
                    gather_y(l, b, z, my_y, y).wait_send()
                    scatter_y(l, b, z, my_y, y).wait_send()
            for y in others_y:
                gather_y(l, b, my_z, my_y, y, own=True).wait_send()
                scatter_y(l, b, my_z, my_y, y).wait_send()
            one_gate(l, b).wait_send()
            for c in range(4):
                one_main(l, b, c).wait_send()
            for x in others_x:
                two_gate(l, b, my_x, x).wait_send()
                for c in range(4):
                    two_main(l, b, c, my_x, x).wait_send()
                across(l, b, my_dp, x * 2 + my_core).wait_send()
            for x in [my_x] + others_x:
                inside(l, b, x * 2 + my_core, x).wait_send()


def store(*refs):
    sem = refs[-1]
    copies = [pltpu.make_async_copy(refs[i], refs[4 + i], sem.at[i]) for i in range(4)]
    for copy in copies:
        copy.start()
    for copy in copies:
        copy.wait()


def per_device(
    tokens,
    lengths,
    norm_gain,
    query_weight,
    key_weight,
    value_weight,
    outgate_weight,
    input_gate_weight,
    forget_gate_weight,
    forget_bias,
    out_weight,
    cell_state,
    norm_state,
    max_state,
):
    n_tp, n_dp = lax.axis_size("tp"), lax.axis_size("dp")
    seq_here, span, feat = tokens.shape
    seqs, heads, size = cell_state.shape[1:4]
    own_rows, rows = seq_here * span // BATCHES, seqs * span // BATCHES
    cols, chips = heads * size, n_dp // 2
    everyone, many = n_tp * own_rows, chips * rows
    n_y = chips if n_tp % chips == 0 else 1
    n_z = n_tp // n_y
    vmem = pl.BlockSpec(memory_space=pltpu.VMEM)
    hbm = pl.BlockSpec(memory_space=pltpu.HBM)
    V, sem = pltpu.VMEM, pltpu.SemaphoreType.DMA
    LB = (LAYERS, BATCHES)
    inputs = {
        "tokens": tokens.reshape(BATCHES, own_rows, feat),
        "lengths_in": lengths,
        "gain_in": norm_gain,
        "weight_q": query_weight,
        "weight_k": key_weight,
        "weight_v": value_weight,
        "weight_o": outgate_weight,
        "weight_in": jnp.swapaxes(input_gate_weight, 1, 2),
        "weight_forget": jnp.swapaxes(forget_gate_weight, 1, 2),
        "bias_in": forget_bias,
        "weight_out": out_weight,
        "cell_in": cell_state,
        "norm_in": norm_state,
        "max_in": jnp.swapaxes(max_state, 1, 2),
    }
    outputs = {
        "tokens_out": V((BATCHES, own_rows, feat), BF16),
        "cells": V(cell_state.shape, F32),
        "norm_out": V(norm_state.shape, F32),
        "max_out": V((LAYERS, heads, seqs), F32),
    }
    scratch = {
        "lengths": pltpu.SMEM(lengths.shape, jnp.int32),
        "gain": V(norm_gain.shape, F32),
        "norm": V(norm_state.shape, F32),
        "stabils": V((LAYERS, heads, seqs), F32),
        "bias": V(forget_bias.shape, F32),
        "current": V((*LB, own_rows, feat), BF16),
        "wts": V((LAYERS, 4, feat, cols), BF16),
        "wgate": V((LAYERS, 2, input_gate_weight.shape[2], feat), BF16),
        "wout": V((LAYERS, cols, feat), BF16),
        "pad": V((LAYERS, seqs + 8, LANES), F32),
        "top_buf": V((LAYERS, seqs, LANES), F32),
        "gate_w": V((LAYERS, LANES, feat), BF16),
        "gathered": V((*LB, everyone, feat), BF16),
        "scaled": V((2, many, feat), BF16),
        "both": V((2, many, cols), F32),
        "own_main": V((BATCHES, 4, many, cols), F32),
        "own_gate": V((BATCHES, 2, many, LANES), F32),
        "send1": V((*LB, 4, many, cols), BF16),
        "send1g": V((*LB, many, LANES), BF16),
        "recv1": V((*LB, 4, many, cols), BF16),
        "recv1g": V((*LB, many, LANES), BF16),
        "send2": V((*LB, 4, many, cols), BF16),
        "send2g": V((*LB, many, LANES), BF16),
        "recv2": V((*LB, 4, chips, rows, cols), BF16),
        "recv2g": V((*LB, chips, rows, LANES), BF16),
        "heads_buf": V((BATCHES, 4, rows, cols), BF16),
        "gated": V((*LB, n_dp, rows, cols), BF16),
        "mixed": V((*LB, everyone, feat), BF16),
        "mixed_s": V((*LB, n_z, own_rows, feat), BF16),
        "mixed_y": V((*LB, n_z, n_y, own_rows, feat), BF16),
        "mixed_in": V((*LB, n_z, own_rows, feat), BF16),
        "load_sem": sem((6 + 8 * LAYERS,)),
        "gat_s": sem((*LB, n_z)),
        "gat_r": sem((*LB, n_z)),
        "gfw_s": sem((*LB, n_z, n_y)),
        "gfw_r": sem((*LB, n_z, n_y)),
        "one_s": sem((*LB, 5)),
        "one_r": sem((*LB, 5)),
        "two_s": sem((*LB, 5, chips)),
        "two_r": sem((*LB, 5, chips)),
        "gg_s": sem((*LB, chips)),
        "gg_r": sem((*LB, chips)),
        "fw_s": sem((*LB, chips)),
        "fw_r": sem((*LB, chips)),
        "mix_s": sem((*LB, n_z)),
        "mix_r": sem((*LB, n_z)),
        "my_s": sem((*LB, n_z, n_y)),
        "my_r": sem((*LB, n_z, n_y)),
    }
    names = (*inputs, *outputs, *scratch)
    result = pl.pallas_call(
        functools.partial(kernel, (n_tp, n_dp, span, heads, size, n_y, names)),
        out_shape=tuple(outputs.values()),
        in_specs=[hbm] * len(inputs),
        out_specs=(vmem,) * len(outputs),
        scratch_shapes=list(scratch.values()),
        compiler_params=pltpu.CompilerParams(
            collective_id=0, has_side_effects=True, vmem_limit_bytes=56 * 1024 * 1024
        ),
    )(*inputs.values())
    result = pl.pallas_call(
        store,
        out_shape=tuple(jax.ShapeDtypeStruct(part.shape, part.dtype) for part in result),
        in_specs=[vmem] * 4,
        out_specs=(pl.BlockSpec(memory_space=pl.ANY),) * 4,
        scratch_shapes=[sem((4,))],
        compiler_params=pltpu.CompilerParams(vmem_limit_bytes=16 * 1024 * 1024),
    )(*result)
    return (result[0].reshape(tokens.shape), *result[1:3], jnp.swapaxes(result[3], 1, 2))


def solution(mesh):
    return jax.shard_map(
        per_device,
        mesh=mesh,
        in_specs=(
            P("tp", None, "dp"),
            P("dp"),
            P(None, "dp"),
            P(None, "dp", "tp"),
            P(None, "dp", "tp"),
            P(None, "dp", "tp"),
            P(None, "dp", "tp"),
            P(),
            P(),
            P(None, "tp"),
            P(None, "tp", "dp"),
            P(None, "dp", "tp", None, None),
            P(None, "dp", "tp", None),
            P(None, "dp", "tp"),
        ),
        out_specs=(
            P("tp", None, "dp"),
            P(None, "dp", "tp", None, None),
            P(None, "dp", "tp", None),
            P(None, "dp", "tp"),
        ),
        check_vma=False,
    )
```

time: 143 us -> 113 us (0.79)
  Pallas kernels: 135 us -> 112 us
  local copies, waits for them, and re-layouts: 6.45 us -> 0 us
    pallas_call x1, Pallas kernels: 133 us -> 110 us  [per_device(): pl.pallas_call(functools.partial(kernel, (n_tp, n_dp, span, heads, size,...]
    unnamed x16 -> x0, local copies, waits for them, and re-layouts: 6.45 us -> none
where the time goes in v2:
time: 113 us
  Pallas kernels  112 us (99%)
    pallas_call x1, Pallas kernels, per_device(): pl.pallas_call(functools.partial(kernel, (n_tp, n_dp, span, heads, size,...  110 us

profile of v2, /device:TPU:0, one launch (start us, length us, event | category | flops | bytes accessed | tf_op | source)
XLA Modules:
  0.0 113.0 jit_solution(12515907000914951914)
XLA Ops:
  0.6 110.3 %shard_map.165 = (bf16[2,32,1024]{2,1,0:T(8,128)(2,1)S(1)}, f32[2,8,4,128,128]{4,3,2,1,0:T(8,128)S(1)}, f32[2,8,4,128]{3,2,1,0:T(4,128)S(1)}, f32[2,4,8]{2,1,0:T(4,128)S(1)}) custom-call(bf16[2,32,1024]{2,1,0:T(8,128)(2,1)} %bitcast.8, s32[8]{0:T(128)} %refs_1_.1, f32[2,1024]{1,0:T(2,128)} %refs_2_.1, bf16[2,1024,512]{2,1,0:T(8,128)(2,1)} %refs_3_.1, ...), custom_call_target="tpu_custom_call" | custom-call | tf_op jit(solution)/shard_map/pallas_call | solution.py:641
  110.9 2.1 %shard_map.166 = (bf16[2,32,1024]{2,1,0:T(8,128)(2,1)}, f32[2,8,4,128,128]{4,3,2,1,0:T(8,128)}, f32[2,8,4,128]{3,2,1,0:T(4,128)}, f32[2,4,8]{2,1,0:T(4,128)}) custom-call(bf16[2,32,1024]{2,1,0:T(8,128)(2,1)S(1)} %get-tuple-element.12.refs_0_, f32[2,8,4,128,128]{4,3,2,1,0:T(8,128)S(1)} %get-tuple-element.13.refs_1_, ...), custom_call_target="tpu_custom_call" | custom-call | tf_op jit(solution)/shard_map/pallas_call | solution.py:651

commit v3 on v2

v3 whole, which is shorter than its diff:
```python
import functools
import types
import jax
import jax.numpy as jnp
from jax import lax
from jax.experimental import pallas as pl
from jax.experimental.pallas import tpu as pltpu
from jax.sharding import PartitionSpec as P

EPSILON = 1e-06
NEG_FILL = -1e30
LANES = 128
HIGH = lax.Precision.HIGHEST
BF16 = jnp.bfloat16
F32 = jnp.float32
MESH = pl.DeviceIdType.MESH
BATCHES = 4
LAYERS = 2
AHEAD = 2
FORWARD, PROJECT, EXCHANGE, ATTEND, UPDATE, RELAY, MIX, FOLD, FINISH = range(9)
ORDER = (
    0, 1, 2, 100, 101, 102, 10, 200, 201, 20, 110, 202, 300, 301, 302, 120,
    30, 210, 50, 130, 60, 220, 310, 70, 150, 71, 320, 160, 230, 72, 170, 330,
    250, 171, 80, 260, 172, 340, 350, 270, 1000, 360, 271, 272, 1001, 40, 1002, 180,
    1100, 370, 1101, 371, 372, 1102, 280, 1010, 380, 1020, 1200, 1110, 1201, 140, 1202, 240,
    1120, 1030, 1300, 1301, 1302, 1210, 1050, 1130, 1060, 1220, 1310, 1150, 1320, 1070, 1230, 1160,
    1071, 1040, 1330, 1250, 1072, 1170, 1171, 1260, 1172, 1140, 1350, 1080, 1360, 1270, 1340, 1271,
    1180, 1272, 1370, 1240, 1371, 1280, 1372, 1380,
)


def plan(n_z):
    result = []
    for entry in ORDER:
        l, b, step, third = entry // 1000, entry // 100 % 10, entry // 10 % 10, entry % 10
        if step in (FORWARD, FOLD):
            count = n_z - 1
            result += [(l, b, step, j) for j in range(third * count // 3, (third + 1) * count // 3)]
        else:
            result.append((l, b, step, 0))
    return result


def pack_squares(block):
    lane = lax.broadcasted_iota(jnp.int32, block.shape, 1)
    square = jnp.sum(jnp.where(lane >= LANES - 3, block, 0.0), axis=1, keepdims=True)
    first = square.astype(BF16).astype(F32)
    rest = square - first
    second = rest.astype(BF16).astype(F32)
    third = rest - second
    block = jnp.where(lane == LANES - 3, first, block)
    block = jnp.where(lane == LANES - 2, second, block)
    return jnp.where(lane == LANES - 1, third, block).astype(BF16)


def flip_bits(value, mask):
    result = value
    bit = 1
    while bit <= mask:
        if mask & bit:
            result = result + bit * (1 - 2 * lax.rem(value // bit, 2))
        bit = bit * 2
    return result


def kernel(sizes, *refs):
    n_tp, n_dp, span, heads, size, n_y, names = sizes
    r = types.SimpleNamespace(**dict(zip(names, refs)))
    lengths, norm, stabils, gain = r.lengths, r.norm, r.stabils, r.gain
    cells, norm_out, max_out, tokens_out = r.cells, r.norm_out, r.max_out, r.tokens_out
    current, wts, wgate, wout = r.current, r.wts, r.wgate, r.wout
    gathered, scaled, gate_w, both = r.gathered, r.scaled, r.gate_w, r.both
    own_gate, own_main, heads_buf = r.own_gate, r.own_main, r.heads_buf
    gated, mixed, top_buf, pad = r.gated, r.mixed, r.top_buf, r.pad
    load_sem = r.load_sem
    chips = n_dp // 2
    n_z = n_tp // n_y
    my_tp, my_dp = lax.axis_index("tp"), lax.axis_index("dp")
    my_x, my_core = my_dp // 2, lax.rem(my_dp, 2)
    peer_core = 1 - my_core
    peer = my_x * 2 + peer_core
    my_z, my_y = my_tp // n_y, lax.rem(my_tp, n_y)
    own_rows, feat = current.shape[2:]
    seqs = cells.shape[1]
    own_part = own_rows // span
    own_seqs = own_part * BATCHES
    ratio = seqs // own_seqs
    seqs_b = seqs // BATCHES
    rows = seqs_b * span
    total_rows = n_dp * rows
    key_scale = size ** (-0.5)

    def load(index, source, target):
        return pltpu.make_async_copy(source, target, load_sem.at[index])

    start = pl.multiple_of(my_dp * feat, feat)
    small = [
        load(0, r.tokens, current.at[0]),
        load(1, r.lengths_in, lengths),
        load(2, r.gain_in, gain),
        load(3, r.norm_in, norm),
        load(4, r.max_in, stabils),
        load(5, r.bias_in, r.bias),
    ]
    big = []
    for l in range(LAYERS):
        part = []
        for i, source in enumerate((r.weight_in, r.weight_forget)):
            part.append(load(6 + 4 * l, source.at[l, :, pl.ds(start, feat)], wgate.at[l, i]))
        for i, source in enumerate((r.weight_q, r.weight_k, r.weight_v, r.weight_o)):
            part.append(load(7 + 4 * l, source.at[l], wts.at[l, i]))
        part.append(load(8 + 4 * l, r.cell_in.at[l], cells.at[l]))
        part.append(load(9 + 4 * l, r.weight_out.at[l], wout.at[l]))
        big.append(part)
    for copy in small + big[0] + big[1]:
        copy.start()

    power = n_z & (n_z - 1) == 0
    peers_y = [(lax.rem(my_y + j, n_y), j - 1, n_y - j - 1) for j in range(1, n_y)]
    peers_x = [(lax.rem(my_x + j, chips), j - 1, chips - j - 1) for j in range(1, chips)]
    if power:
        peers_z = [(flip_bits(my_z, j), j - 1, j - 1) for j in range(1, n_z)]
    else:
        peers_z = [(lax.rem(my_z + j, n_z), j - 1, n_z - j - 1) for j in range(1, n_z)]
    barrier = pltpu.get_barrier_semaphore()
    for y, _, _ in peers_y:
        pl.semaphore_signal(
            barrier, inc=1, device_id={"tp": my_z * n_y + y}, device_id_type=MESH
        )
    for z, _, _ in peers_z:
        pl.semaphore_signal(
            barrier, inc=1, device_id={"tp": z * n_y + my_y}, device_id_type=MESH
        )
    for x, _, _ in peers_x:
        pl.semaphore_signal(
            barrier, inc=1, device_id={"dp": x * 2 + my_core}, device_id_type=MESH
        )
    pl.semaphore_signal(barrier, inc=1, device_id={"dp": peer}, device_id_type=MESH)
    pl.semaphore_wait(barrier, len(peers_y) + len(peers_z) + chips)

    def remote(src, dst, s, rcv, where):
        return pltpu.make_async_remote_copy(
            src_ref=src, dst_ref=dst, send_sem=s, recv_sem=rcv, device_id=where, device_id_type=MESH
        )

    def tp_rows(t):
        return pl.ds(pl.multiple_of(t * own_rows, own_rows), own_rows)

    def x_rows(x):
        return pl.ds(pl.multiple_of(x * rows, rows), rows)

    def drain_sent(ref, sem_ref):
        remote(ref, ref, sem_ref, sem_ref, {"dp": peer}).wait_send()

    def drain_received(ref, sem_ref):
        remote(ref, ref, sem_ref, sem_ref, {"dp": peer}).wait_recv()

    def block_rows(count):
        return pl.ds(0, count * own_rows)

    def gather_z(l, b, peer_z, own=True):
        z, here, there = peer_z
        return remote(
            current.at[l, b],
            gathered.at[l, b, tp_rows((my_z if own else z) * n_y + my_y)],
            r.gat_s.at[b],
            r.gat_r.at[b, there if own else here],
            {"tp": z * n_y + my_y},
        )

    def gather_y(l, b, z, peer_y, own):
        part = gathered.at[l, b, tp_rows(z * n_y + my_y)]
        return remote(
            current.at[l, b] if own else part,
            part,
            r.gat_s.at[b] if own else r.gfw_s.at[b],
            r.gfw_r.at[b],
            {"tp": my_z * n_y + peer_y[0]},
        )

    def one_gate(l, b):
        return remote(
            r.send1g.at[l, b],
            r.recv1g.at[l, b],
            r.one_s.at[b, 1],
            r.one_r.at[b, 4],
            {"dp": peer},
        )

    def one_main(l, b, c):
        return remote(
            r.send1.at[l, b, c],
            r.recv1.at[l, b, c],
            r.one_s.at[b, 0],
            r.one_r.at[b, c],
            {"dp": peer},
        )

    def two_gate(l, b, peer_x):
        x, _, there = peer_x
        return remote(
            r.send2g.at[l, b, x_rows(x)],
            r.recv2g.at[l, b, there],
            r.two_s.at[b, 1],
            r.two_r.at[b, 1],
            {"dp": x * 2 + my_core},
        )

    def two_main(l, b, c, peer_x):
        x, _, there = peer_x
        return remote(
            r.send2.at[l, b, c, x_rows(x)],
            r.recv2.at[l, b, c, there],
            r.two_s.at[b, 0],
            r.two_r.at[b, 0],
            {"dp": x * 2 + my_core},
        )

    def across(l, b, peer_x, own=True):
        x, here, there = peer_x
        part = gated.at[l, b, my_dp if own else x * 2 + my_core]
        return remote(
            part,
            part,
            r.gg_s.at[b],
            r.gg_r.at[b, there if own else here],
            {"dp": x * 2 + my_core},
        )

    def inside(l, b, block):
        part = gated.at[l, b, block]
        return remote(part, part, r.fw_s.at[b], r.fw_r.at[b], {"dp": peer})

    def scatter_y(l, b, z, peer_y):
        y, _, there = peer_y
        return remote(
            mixed.at[l, b, tp_rows(z * n_y + y)],
            r.mixed_y.at[l, b, z, there],
            r.my_s.at[b],
            r.my_r.at[b, z],
            {"tp": my_z * n_y + y},
        )

    def scatter_z(l, b, peer_z):
        z, here, there = peer_z
        return remote(
            r.mixed_s.at[l, b, here],
            r.mixed_in.at[l, b, there],
            r.mix_s.at[b],
            r.mix_r.at[b],
            {"tp": z * n_y + my_y},
        )

    def sent_gather(l, b):
        drain_sent(gathered.at[l, b, block_rows(n_z + n_y - 2)], r.gat_s.at[b])
        drain_sent(gathered.at[l, b, block_rows((n_z - 1) * (n_y - 1))], r.gfw_s.at[b])

    def sent_project(l, b):
        drain_sent(r.send1.at[l, b], r.one_s.at[b, 0])
        drain_sent(r.send1g.at[l, b], r.one_s.at[b, 1])
        drain_sent(r.recv2.at[l, b], r.two_s.at[b, 0])
        drain_sent(r.recv2g.at[l, b], r.two_s.at[b, 1])

    def sent_attend(l, b):
        drain_sent(gated.at[l, b, pl.ds(0, chips - 1)], r.gg_s.at[b])
        drain_sent(gated.at[l, b, pl.ds(0, chips)], r.fw_s.at[b])

    def sent_mix(l, b):
        drain_sent(r.mixed_y.at[l, b], r.my_s.at[b])
        drain_sent(r.mixed_s.at[l, b], r.mix_s.at[b])

    def begin(l, b):
        if l:
            sent_gather(l - 1, b)
        for peer_z in peers_z:
            gather_z(l, b, peer_z).start()
        for peer_y in peers_y:
            gather_y(l, b, my_z, peer_y, own=True).start()
        gathered[l, b, tp_rows(my_tp)] = current[l, b]

    small[0].wait()
    for b in range(BATCHES):
        begin(0, b)
    for copy in small[1:]:
        copy.wait()

    row_id = lax.broadcasted_iota(jnp.int32, (rows, rows), 0)
    col_id = lax.broadcasted_iota(jnp.int32, (rows, rows), 1)
    allowed = (row_id // span == col_id // span) & (col_id <= row_id)
    lane = lax.broadcasted_iota(jnp.int32, (rows, LANES), 1)
    row_l = lax.broadcasted_iota(jnp.int32, (rows, LANES), 0)
    runs = [
        [slice(j * own_seqs + b * own_part, j * own_seqs + (b + 1) * own_part) for j in range(ratio)]
        for b in range(BATCHES)
    ]

    def live_of(b):
        reach = jnp.zeros((rows, LANES), jnp.int32)
        place = 0
        for run in runs[b]:
            for s in range(run.start, run.stop):
                reach = jnp.where(row_l // span == place, lengths[s], reach)
                place = place + 1
        return lax.rem(row_l, span) < reach

    pad[...] = jnp.zeros_like(pad)
    for l in range(LAYERS):
        pad[l, 0:seqs, 0:heads] = jnp.transpose(stabils[l])
        pad[l, seqs : seqs + 1, 0:heads] = r.bias[l : l + 1, :]

    def spread(value):
        wide = jnp.broadcast_to(value[:, None, :], (seqs_b, span, value.shape[-1]))
        return wide.reshape(rows, value.shape[-1])

    def last(value):
        return value.reshape(seqs_b, span, value.shape[-1])[:, span - 1, :]

    arrived = set()

    def arrive(l, first, end):
        if (l, first) not in arrived:
            arrived.add((l, first))
            if end == first + 1:
                big[l][first].wait()
            else:
                whole = wgate.at[l] if first == 0 else wts.at[l]
                load(6 + 4 * l + (first > 0), whole, whole).wait()

    def gate_columns(l):
        arrive(l, 0, 2)
        total_heads = wgate.shape[2]
        pick_r = lax.broadcasted_iota(jnp.int32, (LANES, total_heads), 1)
        pick_c = lax.broadcasted_iota(jnp.int32, (LANES, total_heads), 0)
        head_start = my_tp * heads
        pick_in = ((pick_r == head_start + pick_c) & (pick_c < heads)).astype(F32).astype(BF16)
        pick_fg = (
            ((pick_r == head_start + pick_c - heads) & (pick_c >= heads) & (pick_c < 2 * heads))
            .astype(F32)
            .astype(BF16)
        )
        gate_w[l] = (
            jnp.dot(pick_in, wgate[l, 0], preferred_element_type=F32)
            + jnp.dot(pick_fg, wgate[l, 1], preferred_element_type=F32)
        ).astype(BF16)

    for l in range(LAYERS):
        gate_columns(l)

    def forward(l, b, j):
        gather_z(l, b, peers_z[j], own=False).wait_recv()
        for peer_y in peers_y:
            gather_y(l, b, peers_z[j][0], peer_y, own=False).start()

    def project(l, b):
        if l:
            sent_project(l - 1, b)
        drain_received(gathered.at[l, b, block_rows(n_z * (n_y - 1))], r.gfw_r.at[b])
        gain_row = gain[l : l + 1, :]
        for d in range(n_dp):
            block = gathered[l, b, d * rows : (d + 1) * rows].astype(F32)
            core, x = d % 2, d // 2
            scaled[core, x * rows : (x + 1) * rows] = (block * gain_row).astype(BF16)
            own_gate[b, core, x * rows : (x + 1) * rows] = jnp.broadcast_to(
                jnp.sum(block * block, axis=1, keepdims=True), (rows, LANES)
            )
        lane_all = lax.broadcasted_iota(jnp.int32, (chips * rows, LANES), 1)
        for core in range(2):
            part = lax.dot_general(
                scaled[core], gate_w[l], (((1,), (1,)), ((), ())), preferred_element_type=F32
            )
            own_gate[b, core] = jnp.where(lane_all == LANES - 3, own_gate[b, core], part)
        r.send1g[l, b] = pack_squares(own_gate[b, peer_core])
        one_gate(l, b).start()
        arrive(l, 2, 6)

        def one(c, carry):
            flat = scaled[...].reshape(2 * chips * rows, feat)
            both[...] = jnp.dot(flat, wts[l, c], preferred_element_type=F32).reshape(both.shape)
            r.send1[l, b, c] = both[peer_core].astype(BF16)
            one_main(l, b, c).start()
            own_main[b, c] = both[my_core]

            @pl.when(c == AHEAD)
            def _():
                exchange_gate(l, b)

            @pl.when(c >= AHEAD)
            def _():
                exchange_main(l, b, c - AHEAD)

            return carry

        lax.fori_loop(0, 4, one, 0)

    def exchange_gate(l, b):
        one_gate(l, b).wait_recv()
        summed = own_gate[b, my_core] + r.recv1g[l, b].astype(F32)
        own_gate[b, my_core] = summed
        r.send2g[l, b] = pack_squares(summed)
        for peer_x in peers_x:
            two_gate(l, b, peer_x).start()

    def exchange_main(l, b, c):
        one_main(l, b, c).wait_recv()
        own = own_main[b, c] + r.recv1[l, b, c].astype(F32)
        own_main[b, c] = own
        r.send2[l, b, c] = own.astype(BF16)
        for peer_x in peers_x:
            two_main(l, b, c, peer_x).start()

    def exchange(l, b):
        def one(c, carry):
            exchange_main(l, b, c)
            return carry

        lax.fori_loop(4 - AHEAD, 4, one, 0)

    kept = {}

    def attend(l, b):
        live = live_of(b)
        if l:
            sent_attend(l - 1, b)
        drain_received(r.recv2g.at[l, b], r.two_r.at[b, 1])
        sums = own_gate[b, my_core, x_rows(my_x)]
        for j in range(chips - 1):
            sums = sums + r.recv2g[l, b, j].astype(F32)
        square = jnp.sum(jnp.where(lane >= LANES - 3, sums, 0.0), axis=1, keepdims=True)
        scale = lax.rsqrt(square / (feat * n_dp) + EPSILON)
        gates = scale * sums
        stabil = jnp.concatenate([pad[l, run] for run in runs[b]], axis=0)
        forget = pltpu.roll(gates, LANES - heads, 1) + pad[l, seqs : seqs + 1, :]
        log_forget = jnp.minimum(forget, 0.0) - jnp.log1p(jnp.exp(-jnp.abs(forget)))
        in_gate = jnp.where(live, gates, NEG_FILL)
        log_forget = jnp.where(live, log_forget, 0.0)
        cumul = jnp.dot(
            allowed.astype(F32), log_forget, preferred_element_type=F32, precision=HIGH
        )
        carried = cumul + spread(stabil)
        source = jnp.transpose(in_gate - cumul)
        arrive(l, 6, 7)
        drain_received(r.recv2.at[l, b], r.two_r.at[b, 0])
        for c in range(4):
            full = own_main[b, c, x_rows(my_x)]
            for j in range(chips - 1):
                full = full + r.recv2[l, b, c, j].astype(F32)
            heads_buf[l, b, c] = (scale * full).astype(BF16)

        ids = [s for run in runs[b] for s in range(run.start, run.stop)]
        running = jnp.zeros((rows, LANES), F32)
        for h in range(heads):
            span_h = slice(h * size, (h + 1) * size)
            normer = jnp.concatenate([norm[l, run, h, :] for run in runs[b]], axis=0)
            q, k, v = (heads_buf[l, b, c, :, span_h] for c in range(3))
            weight = jnp.where(allowed, cumul[:, h : h + 1] + source[h : h + 1, :], NEG_FILL)
            top = jnp.maximum(jnp.max(weight, axis=1, keepdims=True), carried[:, h : h + 1])
            running = jnp.where(lane == h, top, running)
            decay = jnp.exp(carried[:, h : h + 1] - top)
            scores = lax.dot_general(
                q, k, (((1,), (1,)), ((), ())), preferred_element_type=F32
            )
            scores = scores * key_scale * jnp.exp(weight - top)
            numer = jnp.dot(scores.astype(BF16), v, preferred_element_type=F32)
            from_cell = jnp.concatenate(
                [
                    jnp.dot(
                        q[i * span : (i + 1) * span],
                        cells[l, s, h].astype(BF16),
                        preferred_element_type=F32,
                    )
                    for i, s in enumerate(ids)
                ],
                axis=0,
            )
            numer = numer + decay * from_cell
            from_norm = jnp.sum(q.astype(F32) * spread(normer), axis=1, keepdims=True)
            denom = jnp.sum(scores, axis=1, keepdims=True) + decay * from_norm
            readout = numer / jnp.maximum(jnp.abs(denom), 1.0)
            readout = jnp.where(live, readout, 0.0)
            outgate = heads_buf[l, b, 3, :, span_h].astype(F32)
            gated[l, b, my_dp, :, span_h] = (readout / (1.0 + jnp.exp(-outgate))).astype(BF16)

        for peer_x in peers_x:
            across(l, b, peer_x).start()
        inside(l, b, my_dp).start()
        kept[l, b] = running, cumul, in_gate, stabil

    def update(l, b):
        running, cumul, in_gate, stabil = kept[l, b]
        ids = [s for run in runs[b] for s in range(run.start, run.stop)]
        top_last, cumul_last = last(running), last(cumul)
        weights = jnp.exp(spread(cumul_last - top_last) - cumul + in_gate)
        fade = jnp.exp(cumul_last + stabil - top_last)
        for j, run in enumerate(runs[b]):
            top_buf[l, run] = top_last[j * own_part : (j + 1) * own_part]
        seq_col = lax.broadcasted_iota(jnp.int32, (size, rows), 1) // span
        pick = (
            lax.broadcasted_iota(jnp.int32, (seqs_b, rows), 1) // span
            == lax.broadcasted_iota(jnp.int32, (seqs_b, rows), 0)
        ).astype(F32)
        for h in range(heads):
            span_h = slice(h * size, (h + 1) * size)
            normer = jnp.concatenate([norm[l, run, h, :] for run in runs[b]], axis=0)
            v = heads_buf[l, b, 2, :, span_h]
            k = heads_buf[l, b, 1, :, span_h].astype(F32) * key_scale * weights[:, h : h + 1]
            flipped = jnp.transpose(k)
            stacked = jnp.concatenate(
                [jnp.where(seq_col == i, flipped, 0.0).astype(BF16) for i in range(seqs_b)], axis=0
            )
            added = jnp.dot(stacked, v, preferred_element_type=F32)
            for i, s in enumerate(ids):
                cells[l, s, h] = (
                    fade[i : i + 1, h : h + 1] * cells[l, s, h]
                    + added[i * size : (i + 1) * size]
                )
            moved = fade[:, h : h + 1] * normer + jnp.dot(
                pick, k, preferred_element_type=F32, precision=HIGH
            )
            for j, run in enumerate(runs[b]):
                norm_out[l, run, h, :] = moved[j * own_part : (j + 1) * own_part]

    def relay(l, b):
        for peer_x in peers_x:
            across(l, b, peer_x, own=False).wait_recv()
            inside(l, b, peer_x[0] * 2 + my_core).start()

    def mix(l, b):
        arrive(l, 7, 8)
        if l:
            sent_mix(l - 1, b)
        drain_received(gated.at[l, b, pl.ds(0, chips)], r.fw_r.at[b])
        flat = gated[l, b].reshape(total_rows, heads * size)
        mixed[l, b] = jnp.dot(flat, wout[l], preferred_element_type=F32).astype(BF16)
        for z in [peer_z[0] for peer_z in peers_z[::-1]] + [my_z]:
            for peer_y in peers_y:
                scatter_y(l, b, z, peer_y).start()

    def folded(l, b, z):
        total = mixed[l, b, tp_rows(z * n_y + my_y), :].astype(F32)
        drain_received(r.mixed_y.at[l, b, z], r.my_r.at[b, z])
        for j in range(n_y - 1):
            total = total + r.mixed_y[l, b, z, j].astype(F32)
        return total

    def fold(l, b, j):
        peer_z = peers_z[::-1][j]
        r.mixed_s[l, b, peer_z[1]] = folded(l, b, peer_z[0]).astype(BF16)
        scatter_z(l, b, peer_z).start()

    def finish(l, b):
        total = folded(l, b, my_z)
        drain_received(r.mixed_in.at[l, b], r.mix_r.at[b])
        for j in range(n_z - 1):
            total = total + r.mixed_in[l, b, j].astype(F32)
        result = (current[l, b].astype(F32) + total).astype(BF16)
        if l == LAYERS - 1:
            tokens_out[b] = result
        else:
            current[l + 1, b] = result
            begin(l + 1, b)

    steps = (forward, project, exchange, attend, update, relay, mix, fold, finish)
    for l, b, step, j in plan(n_z):
        if step in (FORWARD, FOLD):
            steps[step](l, b, j)
        else:
            steps[step](l, b)

    for l in range(LAYERS):
        max_out[l] = jnp.transpose(top_buf[l])[0:heads, :]
    for b in range(BATCHES):
        for sent in (sent_gather, sent_project, sent_attend, sent_mix):
            sent(LAYERS - 1, b)


def store(*refs):
    sem = refs[-1]
    copies = [pltpu.make_async_copy(refs[i], refs[4 + i], sem.at[i]) for i in range(4)]
    for copy in copies:
        copy.start()
    for copy in copies:
        copy.wait()


def per_device(
    tokens,
    lengths,
    norm_gain,
    query_weight,
    key_weight,
    value_weight,
    outgate_weight,
    input_gate_weight,
    forget_gate_weight,
    forget_bias,
    out_weight,
    cell_state,
    norm_state,
    max_state,
):
    n_tp, n_dp = lax.axis_size("tp"), lax.axis_size("dp")
    seq_here, span, feat = tokens.shape
    seqs, heads, size = cell_state.shape[1:4]
    own_rows, rows = seq_here * span // BATCHES, seqs * span // BATCHES
    cols, chips = heads * size, n_dp // 2
    everyone, many = n_tp * own_rows, chips * rows
    n_y = chips if n_tp % chips == 0 else 1
    n_z = n_tp // n_y
    vmem = pl.BlockSpec(memory_space=pltpu.VMEM)
    hbm = pl.BlockSpec(memory_space=pltpu.HBM)
    V, sem = pltpu.VMEM, pltpu.SemaphoreType.DMA
    LB = (LAYERS, BATCHES)
    inputs = dict(
        tokens=tokens.reshape(BATCHES, own_rows, feat),
        lengths_in=lengths,
        gain_in=norm_gain,
        weight_q=query_weight,
        weight_k=key_weight,
        weight_v=value_weight,
        weight_o=outgate_weight,
        weight_in=jnp.swapaxes(input_gate_weight, 1, 2),
        weight_forget=jnp.swapaxes(forget_gate_weight, 1, 2),
        bias_in=forget_bias,
        weight_out=out_weight,
        cell_in=cell_state,
        norm_in=norm_state,
        max_in=jnp.swapaxes(max_state, 1, 2),
    )
    outputs = dict(
        tokens_out=V((BATCHES, own_rows, feat), BF16),
        cells=V(cell_state.shape, F32),
        norm_out=V(norm_state.shape, F32),
        max_out=V((LAYERS, heads, seqs), F32),
    )
    scratch = dict(
        lengths=pltpu.SMEM(lengths.shape, jnp.int32),
        gain=V(norm_gain.shape, F32),
        norm=V(norm_state.shape, F32),
        stabils=V((LAYERS, heads, seqs), F32),
        bias=V(forget_bias.shape, F32),
        current=V((*LB, own_rows, feat), BF16),
        wts=V((LAYERS, 4, feat, cols), BF16),
        wgate=V((LAYERS, 2, input_gate_weight.shape[2], feat), BF16),
        wout=V((LAYERS, cols, feat), BF16),
        pad=V((LAYERS, seqs + 8, LANES), F32),
        top_buf=V((LAYERS, seqs, LANES), F32),
        gate_w=V((LAYERS, LANES, feat), BF16),
        gathered=V((*LB, everyone, feat), BF16),
        scaled=V((2, many, feat), BF16),
        both=V((2, many, cols), F32),
        own_main=V((BATCHES, 4, many, cols), F32),
        own_gate=V((BATCHES, 2, many, LANES), F32),
        send1=V((*LB, 4, many, cols), BF16),
        send1g=V((*LB, many, LANES), BF16),
        recv1=V((*LB, 4, many, cols), BF16),
        recv1g=V((*LB, many, LANES), BF16),
        send2=V((*LB, 4, many, cols), BF16),
        send2g=V((*LB, many, LANES), BF16),
        recv2=V((*LB, 4, chips - 1, rows, cols), BF16),
        recv2g=V((*LB, chips - 1, rows, LANES), BF16),
        heads_buf=V((*LB, 4, rows, cols), BF16),
        gated=V((*LB, n_dp, rows, cols), BF16),
        mixed=V((*LB, everyone, feat), BF16),
        mixed_s=V((*LB, n_z - 1, own_rows, feat), BF16),
        mixed_y=V((*LB, n_z, n_y - 1, own_rows, feat), BF16),
        mixed_in=V((*LB, n_z - 1, own_rows, feat), BF16),
        load_sem=sem((6 + 4 * LAYERS,)),
        gat_s=sem((BATCHES,)),
        gat_r=sem((BATCHES, n_z - 1)),
        gfw_s=sem((BATCHES,)),
        gfw_r=sem((BATCHES,)),
        one_s=sem((BATCHES, 2)),
        one_r=sem((BATCHES, 5)),
        two_s=sem((BATCHES, 2)),
        two_r=sem((BATCHES, 2)),
        gg_s=sem((BATCHES,)),
        gg_r=sem((BATCHES, chips - 1)),
        fw_s=sem((BATCHES,)),
        fw_r=sem((BATCHES,)),
        mix_s=sem((BATCHES,)),
        mix_r=sem((BATCHES,)),
        my_s=sem((BATCHES,)),
        my_r=sem((BATCHES, n_z)),
    )
    names = (*inputs, *outputs, *scratch)
    result = pl.pallas_call(
        functools.partial(kernel, (n_tp, n_dp, span, heads, size, n_y, names)),
        out_shape=tuple(outputs.values()),
        in_specs=[hbm] * len(inputs),
        out_specs=(vmem,) * len(outputs),
        scratch_shapes=list(scratch.values()),
        compiler_params=pltpu.CompilerParams(
            collective_id=0, has_side_effects=True, vmem_limit_bytes=56 * 1024 * 1024
        ),
    )(*inputs.values())
    result = pl.pallas_call(
        store,
        out_shape=tuple(jax.ShapeDtypeStruct(part.shape, part.dtype) for part in result),
        in_specs=[vmem] * 4,
        out_specs=(pl.BlockSpec(memory_space=pl.ANY),) * 4,
        scratch_shapes=[sem((4,))],
        compiler_params=pltpu.CompilerParams(vmem_limit_bytes=16 * 1024 * 1024),
    )(*result)
    return (result[0].reshape(tokens.shape), *result[1:3], jnp.swapaxes(result[3], 1, 2))


def solution(mesh):
    return jax.shard_map(
        per_device,
        mesh=mesh,
        in_specs=(
            P("tp", None, "dp"),
            P("dp"),
            P(None, "dp"),
            P(None, "dp", "tp"),
            P(None, "dp", "tp"),
            P(None, "dp", "tp"),
            P(None, "dp", "tp"),
            P(),
            P(),
            P(None, "tp"),
            P(None, "tp", "dp"),
            P(None, "dp", "tp", None, None),
            P(None, "dp", "tp", None),
            P(None, "dp", "tp"),
        ),
        out_specs=(
            P("tp", None, "dp"),
            P(None, "dp", "tp", None, None),
            P(None, "dp", "tp", None),
            P(None, "dp", "tp"),
        ),
        check_vma=False,
    )
```

time: 113 us -> 87.9 us (0.78)
  Pallas kernels: 112 us -> 86.9 us
    pallas_call x1, Pallas kernels: 110 us -> 84.8 us  [per_device(): pl.pallas_call(functools.partial(kernel, (n_tp, n_dp, span, heads, size,...]
where the time goes in v3:
time: 87.9 us; the launch traced here: 87.7 us
  Pallas kernels  86.9 us (99%)
    pallas_call x1, Pallas kernels, per_device(): pl.pallas_call(functools.partial(kernel, (n_tp, n_dp, span, heads, size,...  84.8 us
    pallas_call x1, Pallas kernels, per_device(): pl.pallas_call(store, out_shape=tuple((jax.ShapeDtypeStruct(part.shape, p...  2.1 us

profile of v3, /device:TPU:0, one launch (start us, length us, event | category | flops | bytes accessed | tf_op | source)
XLA Modules:
  0.0 87.7 jit_solution(7448725066071553886)
XLA Ops:
  0.6 84.8 %shard_map.165 = (bf16[4,16,1024]{2,1,0:T(8,128)(2,1)S(1)}, f32[2,8,4,128,128]{4,3,2,1,0:T(8,128)S(1)}, f32[2,8,4,128]{3,2,1,0:T(4,128)S(1)}, f32[2,4,8]{2,1,0:T(4,128)S(1)}) custom-call(bf16[4,16,1024]{2,1,0:T(8,128)(2,1)} %refs_0_.1, s32[8]{0:T(128)} %refs_1_.1, f32[2,1024]{1,0:T(2,128)} %refs_2_.1, bf16[2,1024,512]{2,1,0:T(8,128)(2,1)} %refs_3_.1, ...), custom_call_target="tpu_custom_call" | custom-call | tf_op jit(solution)/shard_map/pallas_call | solution.py:686
  85.5 2.1 %shard_map.166 = (bf16[4,16,1024]{2,1,0:T(8,128)(2,1)}, f32[2,8,4,128,128]{4,3,2,1,0:T(8,128)}, f32[2,8,4,128]{3,2,1,0:T(4,128)}, f32[2,4,8]{2,1,0:T(4,128)}) custom-call(bf16[4,16,1024]{2,1,0:T(8,128)(2,1)S(1)} %get-tuple-element.12.refs_0_, f32[2,8,4,128,128]{4,3,2,1,0:T(8,128)S(1)} %get-tuple-element.13.refs_1_, ...), custom_call_target="tpu_custom_call" | custom-call | tf_op jit(solution)/shard_map/pallas_call | solution.py:696

commit v4 on v3

--- a/solution.py
+++ b/solution.py
@@ -17,15 +17,15 @@
 BATCHES = 4
 LAYERS = 2
 AHEAD = 2
-FORWARD, PROJECT, EXCHANGE, ATTEND, UPDATE, RELAY, MIX, FOLD, FINISH = range(9)
+FORWARD, PROJECT, EXCHANGE, ATTEND, UPDATE, RELAY, MIX, FOLD, FINISH, GATES = range(10)
 ORDER = (
-    0, 1, 2, 100, 101, 102, 10, 200, 201, 20, 110, 202, 300, 301, 302, 120,
-    30, 210, 50, 130, 60, 220, 310, 70, 150, 71, 320, 160, 230, 72, 170, 330,
-    250, 171, 80, 260, 172, 340, 350, 270, 1000, 360, 271, 272, 1001, 40, 1002, 180,
-    1100, 370, 1101, 371, 372, 1102, 280, 1010, 380, 1020, 1200, 1110, 1201, 140, 1202, 240,
-    1120, 1030, 1300, 1301, 1302, 1210, 1050, 1130, 1060, 1220, 1310, 1150, 1320, 1070, 1230, 1160,
-    1071, 1040, 1330, 1250, 1072, 1170, 1171, 1260, 1172, 1140, 1350, 1080, 1360, 1270, 1340, 1271,
-    1180, 1272, 1370, 1240, 1371, 1280, 1372, 1380,
+    0, 1, 2, 100, 101, 102, 10, 200, 20, 201, 110, 202, 90, 300, 120, 301,
+    302, 30, 190, 210, 50, 130, 220, 60, 310, 150, 290, 70, 40, 320, 71, 160,
+    72, 230, 170, 171, 390, 250, 80, 260, 330, 172, 270, 1000, 350, 271, 360, 272,
+    1001, 1002, 180, 1100, 370, 371, 372, 280, 1101, 1102, 1010, 1020, 380, 1200, 1110, 1201,
+    1202, 1090, 1300, 1120, 1190, 1030, 1301, 1302, 1210, 1130, 1050, 1220, 1310, 1060, 1320, 1150,
+    1290, 1230, 1160, 1390, 1070, 1071, 1240, 1330, 1250, 1170, 1140, 1260, 1040, 1171, 340, 1172,
+    1350, 1072, 1360, 1270, 1340, 1271, 1180, 1272, 1370, 1080, 1371, 1280, 1372, 240, 140, 1380,
 )
 
 
@@ -69,7 +69,7 @@
     lengths, norm, stabils, gain = r.lengths, r.norm, r.stabils, r.gain
     cells, norm_out, max_out, tokens_out = r.cells, r.norm_out, r.max_out, r.tokens_out
     current, wts, wgate, wout = r.current, r.wts, r.wgate, r.wout
-    gathered, scaled, gate_w, both = r.gathered, r.scaled, r.gate_w, r.both
+    gathered, scaled, gate_w = r.gathered, r.scaled, r.gate_w
     own_gate, own_main, heads_buf = r.own_gate, r.own_main, r.heads_buf
     gated, mixed, top_buf, pad = r.gated, r.mixed, r.top_buf, r.pad
     load_sem = r.load_sem
@@ -112,8 +112,7 @@
         part.append(load(8 + 4 * l, r.cell_in.at[l], cells.at[l]))
         part.append(load(9 + 4 * l, r.weight_out.at[l], wout.at[l]))
         big.append(part)
-    for copy in small + big[0] + big[1]:
-        copy.start()
+    small[0].start()
 
     power = n_z & (n_z - 1) == 0
     peers_y = [(lax.rem(my_y + j, n_y), j - 1, n_y - j - 1) for j in range(1, n_y)]
@@ -136,6 +135,8 @@
             barrier, inc=1, device_id={"dp": x * 2 + my_core}, device_id_type=MESH
         )
     pl.semaphore_signal(barrier, inc=1, device_id={"dp": peer}, device_id_type=MESH)
+    for copy in small[1:] + big[0] + big[1]:
+        copy.start()
     pl.semaphore_wait(barrier, len(peers_y) + len(peers_z) + chips)
 
     def remote(src, dst, s, rcv, where):
@@ -359,26 +360,30 @@
         for d in range(n_dp):
             block = gathered[l, b, d * rows : (d + 1) * rows].astype(F32)
             core, x = d % 2, d // 2
-            scaled[core, x * rows : (x + 1) * rows] = (block * gain_row).astype(BF16)
-            own_gate[b, core, x * rows : (x + 1) * rows] = jnp.broadcast_to(
+            role = lax.rem(my_core + core, 2)
+            scaled[role, x * rows : (x + 1) * rows] = (block * gain_row).astype(BF16)
+            own_gate[b, role, x * rows : (x + 1) * rows] = jnp.broadcast_to(
                 jnp.sum(block * block, axis=1, keepdims=True), (rows, LANES)
             )
         lane_all = lax.broadcasted_iota(jnp.int32, (chips * rows, LANES), 1)
-        for core in range(2):
-            part = lax.dot_general(
-                scaled[core], gate_w[l], (((1,), (1,)), ((), ())), preferred_element_type=F32
-            )
-            own_gate[b, core] = jnp.where(lane_all == LANES - 3, own_gate[b, core], part)
-        r.send1g[l, b] = pack_squares(own_gate[b, peer_core])
+        part = lax.dot_general(
+            scaled[...].reshape(2 * chips * rows, feat),
+            gate_w[l],
+            (((1,), (1,)), ((), ())),
+            preferred_element_type=F32,
+        ).reshape(2, chips * rows, LANES)
+        for role in range(2):
+            own_gate[b, role] = jnp.where(lane_all == LANES - 3, own_gate[b, role], part[role])
+        r.send1g[l, b] = pack_squares(own_gate[b, 1])
         one_gate(l, b).start()
         arrive(l, 2, 6)
 
         def one(c, carry):
             flat = scaled[...].reshape(2 * chips * rows, feat)
-            both[...] = jnp.dot(flat, wts[l, c], preferred_element_type=F32).reshape(both.shape)
-            r.send1[l, b, c] = both[peer_core].astype(BF16)
+            both = jnp.dot(flat, wts[l, c], preferred_element_type=F32)
+            r.send1[l, b, c] = both[chips * rows :].astype(BF16)
             one_main(l, b, c).start()
-            own_main[b, c] = both[my_core]
+            own_main[b, c] = both[: chips * rows]
 
             @pl.when(c == AHEAD)
             def _():
@@ -394,8 +399,8 @@
 
     def exchange_gate(l, b):
         one_gate(l, b).wait_recv()
-        summed = own_gate[b, my_core] + r.recv1g[l, b].astype(F32)
-        own_gate[b, my_core] = summed
+        summed = own_gate[b, 0] + r.recv1g[l, b].astype(F32)
+        own_gate[b, 0] = summed
         r.send2g[l, b] = pack_squares(summed)
         for peer_x in peers_x:
             two_gate(l, b, peer_x).start()
@@ -415,29 +420,33 @@
 
         lax.fori_loop(4 - AHEAD, 4, one, 0)
 
-    kept = {}
-
-    def attend(l, b):
+    before, kept = {}, {}
+
+    def gates(l, b):
         live = live_of(b)
-        if l:
-            sent_attend(l - 1, b)
         drain_received(r.recv2g.at[l, b], r.two_r.at[b, 1])
-        sums = own_gate[b, my_core, x_rows(my_x)]
+        sums = own_gate[b, 0, x_rows(my_x)]
         for j in range(chips - 1):
             sums = sums + r.recv2g[l, b, j].astype(F32)
         square = jnp.sum(jnp.where(lane >= LANES - 3, sums, 0.0), axis=1, keepdims=True)
         scale = lax.rsqrt(square / (feat * n_dp) + EPSILON)
-        gates = scale * sums
+        pre = scale * sums
         stabil = jnp.concatenate([pad[l, run] for run in runs[b]], axis=0)
-        forget = pltpu.roll(gates, LANES - heads, 1) + pad[l, seqs : seqs + 1, :]
+        forget = pltpu.roll(pre, LANES - heads, 1) + pad[l, seqs : seqs + 1, :]
         log_forget = jnp.minimum(forget, 0.0) - jnp.log1p(jnp.exp(-jnp.abs(forget)))
-        in_gate = jnp.where(live, gates, NEG_FILL)
+        in_gate = jnp.where(live, pre, NEG_FILL)
         log_forget = jnp.where(live, log_forget, 0.0)
         cumul = jnp.dot(
             allowed.astype(F32), log_forget, preferred_element_type=F32, precision=HIGH
         )
         carried = cumul + spread(stabil)
         source = jnp.transpose(in_gate - cumul)
+        before[l, b] = live, scale, stabil, in_gate, cumul, carried, source
+
+    def attend(l, b):
+        live, scale, stabil, in_gate, cumul, carried, source = before[l, b]
+        if l:
+            sent_attend(l - 1, b)
         arrive(l, 6, 7)
         drain_received(r.recv2.at[l, b], r.two_r.at[b, 0])
         for c in range(4):
@@ -559,7 +568,7 @@
             current[l + 1, b] = result
             begin(l + 1, b)
 
-    steps = (forward, project, exchange, attend, update, relay, mix, fold, finish)
+    steps = (forward, project, exchange, attend, update, relay, mix, fold, finish, gates)
     for l, b, step, j in plan(n_z):
         if step in (FORWARD, FOLD):
             steps[step](l, b, j)
@@ -647,7 +656,6 @@
         gate_w=V((LAYERS, LANES, feat), BF16),
         gathered=V((*LB, everyone, feat), BF16),
         scaled=V((2, many, feat), BF16),
-        both=V((2, many, cols), F32),
         own_main=V((BATCHES, 4, many, cols), F32),
         own_gate=V((BATCHES, 2, many, LANES), F32),
         send1=V((*LB, 4, many, cols), BF16),

time: 87.9 us -> 87 us (0.990)
  Pallas kernels: 86.9 us -> 86 us
    pallas_call x1, Pallas kernels: 84.8 us -> 83.9 us  [per_device(): pl.pallas_call(functools.partial(kernel, (n_tp, n_dp, span, heads, size,...]
where the time goes in v4:
time: 87 us; the launch traced here: 86.8 us
  Pallas kernels  86 us (99%)
    pallas_call x1, Pallas kernels, per_device(): pl.pallas_call(functools.partial(kernel, (n_tp, n_dp, span, heads, size,...  83.9 us
    pallas_call x1, Pallas kernels, per_device(): pl.pallas_call(store, out_shape=tuple((jax.ShapeDtypeStruct(part.shape, p...  2.1 us

profile of v4, /device:TPU:0, one launch (start us, length us, event | category | flops | bytes accessed | tf_op | source)
XLA Modules:
  0.0 86.8 jit_solution(6293028638101131772)
XLA Ops:
  0.6 83.9 %shard_map.165 = (bf16[4,16,1024]{2,1,0:T(8,128)(2,1)S(1)}, f32[2,8,4,128,128]{4,3,2,1,0:T(8,128)S(1)}, f32[2,8,4,128]{3,2,1,0:T(4,128)S(1)}, f32[2,4,8]{2,1,0:T(4,128)S(1)}) custom-call(bf16[4,16,1024]{2,1,0:T(8,128)(2,1)} %refs_0_.1, s32[8]{0:T(128)} %refs_1_.1, f32[2,1024]{1,0:T(2,128)} %refs_2_.1, bf16[2,1024,512]{2,1,0:T(8,128)(2,1)} %refs_3_.1, ...), custom_call_target="tpu_custom_call" | custom-call | tf_op jit(solution)/shard_map/pallas_call | solution.py:694
  84.5 2.1 %shard_map.166 = (bf16[4,16,1024]{2,1,0:T(8,128)(2,1)}, f32[2,8,4,128,128]{4,3,2,1,0:T(8,128)}, f32[2,8,4,128]{3,2,1,0:T(4,128)}, f32[2,4,8]{2,1,0:T(4,128)}) custom-call(bf16[4,16,1024]{2,1,0:T(8,128)(2,1)S(1)} %get-tuple-element.12.refs_0_, f32[2,8,4,128,128]{4,3,2,1,0:T(8,128)S(1)} %get-tuple-element.13.refs_1_, ...), custom_call_target="tpu_custom_call" | custom-call | tf_op jit(solution)/shard_map/pallas_call | solution.py:704
